TPU v7x, 32 devices: a whole 2x2x4 slice. The times are simulated.
32 devices in a mesh: ep: 4 (over y, x), tp: 8 (over z, core).
Axes of the slice: x: 2, y: 2, z: 4, core: 2. Of those that a mesh axis runs over, the one named last changes fastest.
Arguments:
- residual: bfloat16 [128, 2048], P('ep'), may hold values from -20 to 20
- cache_latent: bfloat16 [128, 2048, 256], P(('ep', 'tp')), may hold values from -12 to 12
- cache_rope: bfloat16 [128, 32, 2048], P(('ep', 'tp')), may hold values from -6 to 6
- lengths: int32 [128], P(('ep', 'tp')), may hold values from 2 to 2048, as said below
- query_latent: bfloat16 [128, 32, 256], P(('ep', 'tp')), may hold values from -250 to 250
- query_rope: bfloat16 [128, 32, 32], P(('ep', 'tp')), may hold values from -6 to 6
- norm_gain: bfloat16 [2048], replicated, may hold values from 0.099609375 to 1.8984375
- latent_weight: bfloat16 [2048, 256], replicated, may hold values from -0.125 to 0.125
- latent_gain: bfloat16 [256], replicated, may hold values from 0.099609375 to 1.8984375
- rope_weight: bfloat16 [32, 2048], replicated, may hold values from -0.125 to 0.125
- value_weight: bfloat16 [256, 2048], replicated, may hold values from -0.375 to 0.375
- out_weight: bfloat16 [2048, 2048], P('tp'), may hold values from -1 to 1
- mixer_gain: bfloat16 [2048], replicated, may hold values from 0.099609375 to 1.8984375
- group_router: bfloat16 [2048, 4], replicated, may hold values from -0.0625 to 0.0625
- expert_router: bfloat16 [2048, 8], replicated, may hold values from -0.0625 to 0.0625
- expert_ids: int32 [128, 2], P('ep'), may hold values from 0 to 7, as said below
- gate_weight: bfloat16 [8, 2048, 4096], P('ep', None, 'tp'), may hold values from -0.125 to 0.125
- up_weight: bfloat16 [8, 2048, 4096], P('ep', None, 'tp'), may hold values from -0.125 to 0.125
- down_weight: bfloat16 [8, 4096, 2048], P('ep', 'tp'), may hold values from -0.75 to 0.75
Outputs:
- mixed: bfloat16 [128, 2048], P('ep')
- new_latent: bfloat16 [128, 256], P(('ep', 'tp'))
- new_rope_key: bfloat16 [128, 32], P(('ep', 'tp'))
Inputs may be any that keep to these rules, and one draw needn't show every extreme that they name: `lengths`: every sequence has 2 or more cached positions, and in every draw some sequence has all 2048. `expert_ids`: each row names 2 different experts of one group; group g holds experts g * 2 to g * 2 + 1. Among the rows of one index of ep (aligned blocks of 32 rows) no expert is named more than 16 times, and in every draw some expert is named exactly 16 times in every block.
All inputs are finite; a program needn't handle non-finite values.
Results may differ from a plain program's by a relative error of at most 0.012.
Values may be sent and summed in bfloat16 or wider, within the bound.
A program may use at most 64 MiB of HBM per device.

v0:
```python
import jax
import jax.numpy as jnp
from jax import lax
from jax.sharding import PartitionSpec as P

H = 32
KV = 256
ROPE = 32
NOPE = 64
V = 64
GROUPS = 4
TOPK = 2


NORM_EPSILON = 1e-06
ROPE_BASE = 10000.0


def inverse_rms(values):
    return lax.rsqrt(jnp.mean(values * values, axis=-1, keepdims=True) + NORM_EPSILON)


def rotate(vector, position):
    half_width = vector.shape[-1] // 2
    frequency = ROPE_BASE ** (
        -jnp.arange(0, vector.shape[-1], 2, dtype=jnp.float32) / vector.shape[-1]
    )
    angles = position[..., None] * frequency
    lower_half = vector[..., :half_width]
    upper_half = vector[..., half_width:]
    return jnp.concatenate(
        [
            lower_half * jnp.cos(angles) - upper_half * jnp.sin(angles),
            upper_half * jnp.cos(angles) + lower_half * jnp.sin(angles),
        ],
        axis=-1,
    )


def dispatch_table(expert_rows, experts, capacity):
    flat_ids = expert_rows.reshape(-1)
    hit_table = (flat_ids[:, None] == jnp.arange(experts, dtype=jnp.int32)[None, :]).astype(
        jnp.int32
    )
    slot_rank = jnp.sum((jnp.cumsum(hit_table, axis=0) - hit_table) * hit_table, axis=1)
    slot_index = flat_ids * capacity + slot_rank
    picked = (
        slot_index[None, :] == jnp.arange(experts * capacity, dtype=jnp.int32)[:, None]
    ).astype(jnp.float32)
    return picked.reshape(experts * capacity, expert_rows.shape[0], expert_rows.shape[1])


def route_weights(expert_in, group_router, expert_router, expert_ids, per_group):
    group_logits = jnp.dot(expert_in, group_router, preferred_element_type=jnp.float32)
    expert_logits = jnp.dot(expert_in, expert_router, preferred_element_type=jnp.float32)
    chosen = expert_ids[:, 0] // per_group
    group_hit = (
        jnp.arange(group_logits.shape[1], dtype=jnp.int32)[None, :] == chosen[:, None]
    ).astype(jnp.float32)
    chosen_logit = jnp.sum(group_logits * group_hit, axis=1, keepdims=True)
    group_share = 1.0 / jnp.sum(jnp.exp(group_logits - chosen_logit), axis=1)
    expert_hit = (
        expert_ids[:, :, None] == jnp.arange(expert_logits.shape[1], dtype=jnp.int32)[None, None, :]
    ).astype(jnp.float32)
    picked_logit = jnp.sum(expert_hit * expert_logits[:, None, :], axis=2)
    inner_share = 1.0 / jnp.sum(
        jnp.exp(picked_logit[:, None, :] - picked_logit[:, :, None]), axis=2
    )
    return group_share[:, None] * inner_share


def on_device(
    residual,
    cache_latent,
    cache_rope,
    lengths,
    query_latent,
    query_rope,
    norm_gain,
    latent_weight,
    latent_gain,
    rope_weight,
    value_weight,
    out_weight,
    mixer_gain,
    group_router,
    expert_router,
    expert_ids,
    gate_weight,
    up_weight,
    down_weight,
):
    ep_count = lax.axis_size("ep")
    seq_count = cache_latent.shape[0]
    group_rows = residual.shape[0]
    model_width = residual.shape[1]
    resid_f = residual.astype(jnp.float32)
    own_rows = lax.dynamic_slice_in_dim(resid_f, lax.axis_index("tp") * seq_count, seq_count, 0)
    normed = (own_rows * inverse_rms(own_rows) * norm_gain.astype(jnp.float32)).astype(jnp.bfloat16)
    latent_raw = jnp.dot(normed, latent_weight, preferred_element_type=jnp.float32)
    new_latent = (latent_raw * inverse_rms(latent_raw) * latent_gain.astype(jnp.float32)).astype(
        jnp.bfloat16
    )
    positions = lengths.astype(jnp.float32)
    rope_raw = jnp.dot(normed, rope_weight.T, preferred_element_type=jnp.float32)
    new_rope_key = rotate(rope_raw, positions).astype(jnp.bfloat16)
    query_turned = rotate(query_rope.astype(jnp.float32), positions[:, None]).astype(jnp.bfloat16)
    score_scale = (NOPE + ROPE) ** (-0.5)
    cached = (
        jnp.einsum("shc,spc->shp", query_latent, cache_latent, preferred_element_type=jnp.float32)
        + jnp.einsum("shr,srp->shp", query_turned, cache_rope, preferred_element_type=jnp.float32)
    ) * score_scale
    keeping = (
        jnp.arange(cache_latent.shape[1], dtype=jnp.int32)[None, None, :] < lengths[:, None, None]
    )
    cached = jnp.where(keeping, cached, -jnp.inf)
    fresh = (
        jnp.einsum("shc,sc->sh", query_latent, new_latent, preferred_element_type=jnp.float32)
        + jnp.einsum("shr,sr->sh", query_turned, new_rope_key, preferred_element_type=jnp.float32)
    ) * score_scale
    row_top = jnp.maximum(jnp.max(cached, axis=2), fresh)
    cached_exp = jnp.exp(cached - row_top[:, :, None])
    fresh_exp = jnp.exp(fresh - row_top)
    denominator = jnp.sum(cached_exp, axis=2) + fresh_exp
    cached_weight = (cached_exp / denominator[:, :, None]).astype(jnp.bfloat16)
    fresh_weight = (fresh_exp / denominator).astype(jnp.bfloat16)
    mixed_latent = (
        jnp.einsum("shp,spc->shc", cached_weight, cache_latent, preferred_element_type=jnp.float32)
        + fresh_weight.astype(jnp.float32)[:, :, None] * new_latent.astype(jnp.float32)[:, None, :]
    ).astype(jnp.bfloat16)
    head_values = jnp.einsum(
        "shc,chv->shv",
        mixed_latent,
        value_weight.reshape(KV, H, V),
        preferred_element_type=jnp.float32,
    ).astype(jnp.bfloat16)
    by_heads = lax.all_to_all(head_values, "tp", split_axis=1, concat_axis=0, tiled=True)
    head_terms = jnp.dot(
        by_heads.reshape(group_rows, -1), out_weight, preferred_element_type=jnp.float32
    )
    attended = lax.psum(head_terms, "tp")
    after_attention = (resid_f + attended).astype(jnp.bfloat16)
    after_f = after_attention.astype(jnp.float32)
    expert_in = (after_f * inverse_rms(after_f) * mixer_gain.astype(jnp.float32)).astype(
        jnp.bfloat16
    )
    experts = expert_router.shape[1]
    capacity = 2 * group_rows * TOPK // experts
    route_weight = route_weights(
        expert_in, group_router, expert_router, expert_ids, experts // GROUPS
    )
    picked = dispatch_table(expert_ids, experts, capacity)
    select_rows = jnp.sum(picked, axis=2).astype(jnp.bfloat16)
    outbound = jnp.dot(select_rows, expert_in, preferred_element_type=jnp.float32).astype(
        jnp.bfloat16
    )
    outbound = outbound.reshape(ep_count, gate_weight.shape[0], capacity, model_width)
    rows = lax.all_to_all(outbound, "ep", split_axis=0, concat_axis=0, tiled=True)
    gate_value = jnp.einsum("secd,edf->secf", rows, gate_weight, preferred_element_type=jnp.float32)
    up_value = jnp.einsum("secd,edf->secf", rows, up_weight, preferred_element_type=jnp.float32)
    activation = (jax.nn.silu(gate_value) * up_value).astype(jnp.bfloat16)
    expert_terms = jnp.einsum(
        "secf,efd->secd", activation, down_weight, preferred_element_type=jnp.float32
    )
    combine = jnp.sum(picked * route_weight[None, :, :], axis=2).T
    summed_terms = lax.psum_scatter(expert_terms, "tp", scatter_dimension=3, tiled=True)
    returned_terms = lax.all_to_all(summed_terms, "ep", split_axis=0, concat_axis=0, tiled=True)
    share_width = returned_terms.shape[3]
    moe_part = jnp.dot(
        combine, returned_terms.reshape(-1, share_width), precision=lax.Precision.HIGHEST
    )
    after_cols = lax.dynamic_slice_in_dim(
        after_f, lax.axis_index("tp") * share_width, share_width, 1
    )
    mixed_share = (after_cols + moe_part).astype(jnp.bfloat16)
    mixed = lax.all_gather(mixed_share, "tp", axis=1, tiled=True)
    return (mixed, new_latent, new_rope_key)


def solution(mesh):
    in_specs = (
        P("ep", None),
        P(("ep", "tp"), None, None),
        P(("ep", "tp"), None, None),
        P(("ep", "tp")),
        P(("ep", "tp"), None, None),
        P(("ep", "tp"), None, None),
        P(),
        P(),
        P(),
        P(),
        P(),
        P("tp", None),
        P(),
        P(),
        P(),
        P("ep", None),
        P("ep", None, "tp"),
        P("ep", None, "tp"),
        P("ep", "tp", None),
    )
    out_specs = (P("ep", None), P(("ep", "tp"), None), P(("ep", "tp"), None))
    return jax.shard_map(
        on_device, mesh=mesh, in_specs=in_specs, out_specs=out_specs, check_vma=False
    )
```

profile of v0, /device:TPU:0, one launch (start us, length us, event | category | flops | bytes accessed | tf_op | source)
XLA Modules:
  0.0 177.1 jit_solution(6395437696958432695)
XLA Ops:
  7.2 0.8 convert_element_type.79
  8.0 0.7 iota_compare_fusion.2
  8.7 0.9 convert_element_type.77
  9.8 0.7 convert_element_type.80
  10.5 0.8 convert_element_type.78
  11.3 1.1 fusion.50
  12.4 1.6 multiply_reduce_fusion.2
  14.0 0.7 convert_element_type.82
  14.7 3.5 %fusion.58 = f32[4,32,2048]{2,1,0:T(8,128)S(1)} fusion(bf16[4,32,256]{2,1,0:T(8,128)(2,1)} %param.23, bf16[4,2048,256]{2,1,0:T(8,128)(2,1)} %param.20), kind=kOutput, calls=%fused_computation.90 | convolution fusion | flops 134217728 | bytes 5308416 | tf_op jit(solution)/shard_map/shc,spc->shp/dot_general | solution.py:110
  18.7 0.2 fusion.39
  18.9 0.5 fusion.54
  19.4 0.3 fusion.26
  19.8 1.5 copy.61
  21.3 3.1 %fusion.23 = bf16[4,32,256]{2,1,0:T(8,128)(2,1)S(1)} fusion(bf16[4,2048,256]{2,1,0:T(8,128)(2,1)} %param.20, f32[4,32,2048]{2,1,0:T(8,128)S(1)} %get-tuple-element.18, f32[4,32]{1,0:T(4,128)S(1)} %get-tuple-element.12, f32[4,32]{1,0:T(4,128)S(1)} %fusion.44, f32[4,256]{1,0:T(4,128)S(1)} %get-tuple-element.7, f32[4,32]{1,0:T(4,128)S(1)} %get-tuple-element.11), kind=kOutput, calls=%fused_computation.16 | convolution fusion | flops 135102464 | bytes 5314048 | tf_op jit(solution)/shard_map/shp,spc->shc/dot_general | solution.py:128
  24.4 0.4 fusion.55
  24.8 0.7 reshape.194
  25.5 6.4 %all-to-all-start = ((bf16[8,2,512]{2,1,0:T(2,128)(2,1)}), bf16[8,2,512]{2,1,0:T(2,128)(2,1)S(1)}, u32[]{:S(2)}, u32[]{:S(2)}) async-start(bf16[8,2,512]{2,1,0:T(2,128)(2,1)} %reshape.194), calls=%async_computation | async-start | bytes 32768 | tf_op jit(solution)/shard_map/all_to_all | solution.py:137
  32.7 4.8 %all-to-all-done = bf16[8,2,512]{2,1,0:T(2,128)(2,1)S(1)} async-done(((bf16[8,2,512]{2,1,0:T(2,128)(2,1)}), bf16[8,2,512]{2,1,0:T(2,128)(2,1)S(1)}, u32[]{:S(2)}, u32[]{:S(2)}) %all-to-all-start) | async-done | bytes 16416 | tf_op jit(solution)/shard_map/all_to_all | solution.py:137
  37.7 1.0 fusion.59
  38.8 53.8 %all-reduce.2.cloned.1.call-done = f32[32,2048]{1,0:T(8,128)} async-done(((f32[32,2048]{1,0:T(8,128)}), f32[32,2048]{1,0:T(8,128)}) %all-reduce.2.cloned.1.call-update) | async-done | bytes 262160 | tf_op jit(solution)/shard_map/psum | solution.py:141
  92.6 1.1 multiply_reduce_fusion
  94.3 0.3 convolution_convert_fusion
  94.6 10.6 %all_to_all.25 = bf16[4,2,16,2048]{3,2,1,0:T(8,128)(2,1)S(1)} all-to-all(bf16[4,2,16,2048]{3,2,1,0:T(8,128)(2,1)S(1)} %bitcast.81), channel_id=1, replica_groups=mesh['ep'=4,'tp'=8] {'ep'}, dimensions={0} | all-to-all | bytes 1048576 | tf_op jit(solution)/shard_map/all_to_all | solution.py:158
  105.2 3.0 %fusion.11 = f32[4,2,16,512]{3,2,0,1:T(8,128)S(1)} fusion(bf16[2,2048,512]{2,1,0:T(8,128)(2,1)} %param.35, bf16[4,2,16,2048]{3,2,1,0:T(8,128)(2,1)S(1)} %all_to_all.25), kind=kOutput, calls=%fused_computation.11 | convolution fusion | flops 268435456 | bytes 4980736 | tf_op jit(solution)/shard_map/secd,edf->secf/dot_general | solution.py:159
  108.2 6.0 %fusion.6 = f32[4,2,16,2048]{3,2,0,1:T(8,128)} fusion(bf16[2,512,2048]{2,1,0:T(8,128)(2,1)} %param.37, bf16[2,2048,512]{2,1,0:T(8,128)(2,1)} %param.36, bf16[4,2,16,2048]{3,2,1,0:T(8,128)(2,1)S(1)} %all_to_all.25, f32[4,2,16,512]{3,2,0,1:T(8,128)S(1)} %fusion.11), kind=kOutput, calls=%fused_computation.6 | convolution fusion | flops 537264128 | bytes 10223616 | tf_op jit(solution)/shard_map/secf,efd->secd/dot_general | solution.py:162
  114.3 30.9 %reduce-scatter.2.cloned.1.call-done = f32[4,2,16,256]{3,2,0,1:T(8,128)} async-done(((f32[4,2,16,2048]{3,2,0,1:T(8,128)}), f32[4,2,16,256]{3,2,0,1:T(8,128)}) %reduce-scatter.2.cloned.1.call-update) | async-done | bytes 131088 | tf_op jit(solution)/shard_map/reduce_scatter | solution.py:166
  145.2 1.6 copy.68
  146.8 3.7 %all-to-all-start.2 = ((f32[4,2,16,256]{3,2,1,0:T(8,128)}), f32[4,2,16,256]{3,2,1,0:T(8,128)S(1)}, u32[]{:S(2)}, u32[]{:S(2)}) async-start(f32[4,2,16,256]{3,2,1,0:T(8,128)} %copy.68), calls=%async_computation.3 | async-start | bytes 262144 | tf_op jit(solution)/shard_map/all_to_all | solution.py:167
  150.4 0.6 pad_maximum_fusion.3
  151.1 4.4 %all-to-all-done.2 = f32[4,2,16,256]{3,2,1,0:T(8,128)S(1)} async-done(((f32[4,2,16,256]{3,2,1,0:T(8,128)}), f32[4,2,16,256]{3,2,1,0:T(8,128)S(1)}, u32[]{:S(2)}, u32[]{:S(2)}) %all-to-all-start.2) | async-done | bytes 131104 | tf_op jit(solution)/shard_map/all_to_all | solution.py:167
  155.6 14.0 %all_gather.3 = bf16[32,2048]{1,0:T(8,128)(2,1)S(1)} all-gather(bf16[32,256]{1,0:T(8,128)(2,1)S(1)} %fusion.25), channel_id=1, replica_groups=mesh['ep'=4,'tp'=8] {'tp'}, dimensions={1}, use_global_device_ids=true | all-gather | bytes 147456 | tf_op jit(solution)/shard_map/all_gather | solution.py:176
  169.6 0.7 copy.94
  (57 shorter events, 2.6 us)
Async XLA Ops:
  7.2 30.6 %copy-start = (bf16[256,2048]{1,0:T(8,128)(2,1)S(1)}, bf16[256,2048]{1,0:T(8,128)(2,1)}, u32[]{:S(2)}) copy-start(bf16[256,2048]{1,0:T(8,128)(2,1)} %param.30) | copy-start | bytes 3145732
  7.2 11.1 %copy-start.3 = (bf16[4,32,256]{2,1,0:T(8,128)(2,1)S(1)}, bf16[4,32,256]{2,1,0:T(8,128)(2,1)}, u32[]{:S(2)}) copy-start(bf16[4,32,256]{2,1,0:T(8,128)(2,1)} %param.23) | copy-start | bytes 196612
  7.2 11.7 %copy-start.2 = (bf16[4,32,2048]{2,1,0:T(8,128)(2,1)S(1)}, bf16[4,32,2048]{2,1,0:T(8,128)(2,1)}, u32[]{:S(2)}) copy-start(bf16[4,32,2048]{2,1,0:T(8,128)(2,1)} %param.21) | copy-start | bytes 1572868
  18.3 6.1 %copy-start.7 = (bf16[4,256]{1,0:T(4,128)(2,1)}, bf16[4,256]{1,0:T(4,128)(2,1)S(1)}, u32[]{:S(2)}) copy-start(bf16[4,256]{1,0:T(4,128)(2,1)S(1)} %get-tuple-element.27) | copy-start | bytes 6148
  21.2 10.7 %copy-start.5 = (s32[32,2]{0,1:T(2,128)S(1)}, s32[32,2]{0,1:T(2,128)}, u32[]{:S(2)}) copy-start(s32[32,2]{0,1:T(2,128)} %param.34) | copy-start | bytes 772
  21.3 11.4 %copy-start.6 = (bf16[2048]{0:T(1024)(128)(2,1)S(1)}, bf16[2048]{0:T(1024)(128)(2,1)}, u32[]{:S(2)}) copy-start(bf16[2048]{0:T(1024)(128)(2,1)} %param.31) | copy-start | bytes 12292
  21.3 71.3 %copy-start.1 = (bf16[32,2048]{1,0:T(8,128)(2,1)S(1)}, bf16[32,2048]{1,0:T(8,128)(2,1)}, u32[]{:S(2)}) copy-start(bf16[32,2048]{1,0:T(8,128)(2,1)} %param.19) | copy-start | bytes 393220
  21.3 72.5 %copy-start.8 = (bf16[2048,4]{0,1:T(4,128)(2,1)S(1)}, bf16[2048,4]{0,1:T(4,128)(2,1)}, u32[]{:S(2)}) copy-start(bf16[2048,4]{0,1:T(4,128)(2,1)} %param.32) | copy-start | bytes 49156
  21.3 72.7 %copy-start.4 = (bf16[2048,8]{0,1:T(8,128)(2,1)S(1)}, bf16[2048,8]{0,1:T(8,128)(2,1)}, u32[]{:S(2)}) copy-start(bf16[2048,8]{0,1:T(8,128)(2,1)} %param.33) | copy-start | bytes 98308
  25.5 12.0 %all-to-all-start = ((bf16[8,2,512]{2,1,0:T(2,128)(2,1)}), bf16[8,2,512]{2,1,0:T(2,128)(2,1)S(1)}, u32[]{:S(2)}, u32[]{:S(2)}) async-start(bf16[8,2,512]{2,1,0:T(2,128)(2,1)} %reshape.194), calls=%async_computation | async-start | bytes 32768 | tf_op jit(solution)/shard_map/all_to_all | solution.py:137
  31.9 60.7 %all-reduce.2.cloned.1.call-start = ((), (), s32[]{:S(2)}) async-start(), calls=%async_computation.4 | async-start | bytes 524288 | tf_op jit(solution)/shard_map/psum | solution.py:141
  38.7 106.5 %reduce-scatter.2.cloned.1.call-start = ((), (), s32[]{:S(2)}) async-start(), calls=%async_computation.5 | async-start | bytes 1179648 | tf_op jit(solution)/shard_map/reduce_scatter | solution.py:166
  146.8 8.7 %all-to-all-start.2 = ((f32[4,2,16,256]{3,2,1,0:T(8,128)}), f32[4,2,16,256]{3,2,1,0:T(8,128)S(1)}, u32[]{:S(2)}, u32[]{:S(2)}) async-start(f32[4,2,16,256]{3,2,1,0:T(8,128)} %copy.68), calls=%async_computation.3 | async-start | bytes 262144 | tf_op jit(solution)/shard_map/all_to_all | solution.py:167
Sparse Core Ops, SparseCore 0:
  38.9 53.6 all-reduce.1
  114.4 30.7 reduce-scatter.1
where the time goes:
time: 178 us; the launch traced here: 177 us
  waiting for transfers between devices  93.9 us (53%)
  blocking collectives  24.5 us (14%)
  matrix products  21.4 us (12%)
  between operations  14.3 us (8%)
  starting transfers between devices  10.1 us (6%)
  other arithmetic  7.81 us (4%)
  local copies, waits for them, and re-layouts  5.06 us (3%)
    psum x1, waiting for transfers between devices, on_device(): attended = lax.psum(head_terms, 'tp')  53.8 us
    reduce_scatter x1, waiting for transfers between devices, on_device(): lax.psum_scatter(expert_terms, 'tp', scatter_dimension=3, tiled=True)  30.9 us
    all_gather x1, blocking collectives, on_device(): mixed = lax.all_gather(mixed_share, 'tp', axis=1, tiled=True)  14 us
    all_to_all x1, blocking collectives, on_device(): lax.all_to_all(outbound, 'ep', split_axis=0, concat_axis=0, tiled=True)  10.6 us
    all_to_all x1, starting transfers between devices, on_device(): lax.all_to_all(head_values, 'tp', split_axis=1, concat_axis=0, tiled=True)  6.35 us
    dot_general x1, matrix products, on_device(): jnp.einsum('secf,efd->secd', activation, down_weight, preferred_element_t...  6.04 us
    all_to_all x1, waiting for transfers between devices, on_device(): lax.all_to_all(head_values, 'tp', split_axis=1, concat_axis=0, tiled=True)  4.83 us
    all_to_all x1, waiting for transfers between devices, on_device(): lax.all_to_all(summed_terms, 'ep', split_axis=0, concat_axis=0, tiled=True)  4.38 us
  transfers between devices with their start and end apart: 4, of which 4 were waited for; matrix products, arithmetic and copies ran while one was open for 1% of the time, Pallas kernels for 0%

commit v1 on v0

v1 whole, which is shorter than its diff:
```python
import functools

import jax
import jax.numpy as jnp
from jax import lax
from jax.experimental import pallas as pl
from jax.experimental.pallas import tpu as pltpu
from jax.sharding import PartitionSpec as P

NORM_EPSILON = 1e-06
ROPE_BASE = 10000.0
TOPK = 2

F32 = jnp.float32
BF16 = jnp.bfloat16


def dot(a, b, contract=((1,), (0,)), precision=None):
    return lax.dot_general(
        a, b, (contract, ((), ())), preferred_element_type=F32, precision=precision
    )


def inverse_rms(values):
    return lax.rsqrt(jnp.mean(values * values, axis=-1, keepdims=True) + NORM_EPSILON)


def iota(shape, dim):
    return lax.broadcasted_iota(jnp.int32, shape, dim)


def layer(
    sizes,
    residual,
    cache_latent,
    cache_rope,
    lengths,
    query_latent,
    query_rope,
    norm_gain,
    latent_weight,
    latent_gain,
    rope_weight,
    value_weight,
    out_weight,
    mixer_gain,
    group_router,
    expert_router,
    expert_ids,
    gate_weight,
    up_weight,
    down_weight,
    mixed_out,
    latent_out,
    rope_out,
    residual_v,
    cache_v,
    rope_v,
    query_v,
    query_rope_v,
    norm_gain_v,
    latent_weight_v,
    latent_gain_v,
    rope_weight_v,
    value_v,
    out_v,
    mixer_gain_v,
    group_router_v,
    expert_router_v,
    ids_v,
    gate_v,
    up_v,
    down_v,
    head_send,
    head_recv,
    meta_send,
    meta_recv,
    sum_send,
    sum_recv,
    disp_send,
    disp_recv,
    ret_send,
    ret_recv,
    share_send,
    share_recv,
    load_sem,
    cache_sem,
    rope_sem,
    expert_sem,
    head_sems,
    meta_sems,
    sum_sems,
    disp_sems,
    ret_sems,
    share_sems,
):
    n_ep, n_tp, slots, scale = sizes
    n_dev = n_ep * n_tp
    rows, width = residual_v.shape
    seqs, heads, latent = query_v.shape
    rope_width = rope_weight_v.shape[0]
    half = rope_width // 2
    length = cache_v.shape[1]
    pad = head_send.shape[1]
    head_cols = head_send.shape[2]
    col = width // n_tp
    local_experts = gate_v.shape[0]
    experts = expert_router_v.shape[0]
    groups = group_router_v.shape[0]
    per_group = experts // groups
    value_dim = value_v.shape[1] // heads

    my_e = lax.axis_index("ep")
    my_t = lax.axis_index("tp")
    me = my_e * n_tp + my_t

    loads = [
        pltpu.make_async_copy(src, dst, load_sem.at[i])
        for i, (src, dst) in enumerate(
            [
                (residual, residual_v),
                (norm_gain, norm_gain_v),
                (latent_weight, latent_weight_v),
                (latent_gain, latent_gain_v),
                (rope_weight, rope_weight_v),
                (query_rope, query_rope_v),
                (query_latent, query_v),
                (expert_ids, ids_v),
                (value_weight, value_v),
                (out_weight, out_v),
                (mixer_gain, mixer_gain_v),
                (group_router, group_router_v),
                (expert_router, expert_router_v),
            ]
        )
    ]
    caches = [
        pltpu.make_async_copy(cache_latent.at[s], cache_v.at[s], cache_sem.at[s])
        for s in range(seqs)
    ]
    ropes = [
        pltpu.make_async_copy(cache_rope.at[s], rope_v.at[s], rope_sem.at[s])
        for s in range(seqs)
    ]
    expert_loads = [
        [
            pltpu.make_async_copy(src.at[l], dst.at[l], expert_sem.at[k, l])
            for l in range(local_experts)
        ]
        for k, (src, dst) in enumerate(
            [(gate_weight, gate_v), (up_weight, up_v), (down_weight, down_v)]
        )
    ]
    for load in loads[:8]:
        load.start()
    for s in range(seqs):
        ropes[s].start()
        caches[s].start()
    for load in loads[8:]:
        load.start()
    for kind in expert_loads:
        for load in kind:
            load.start()

    barrier = pltpu.get_barrier_semaphore()

    def device(t):
        return {"ep": t // n_tp, "tp": lax.rem(t, n_tp)}

    def greet(i, carry):
        pl.semaphore_signal(
            barrier,
            inc=1,
            device_id=device(lax.rem(me + i, n_dev)),
            device_id_type=pl.DeviceIdType.MESH,
        )
        return carry

    lax.fori_loop(1, n_dev, greet, 0)

    def remote(src, dst, send_sem, recv_sem, e, t):
        return pltpu.make_async_remote_copy(
            src_ref=src,
            dst_ref=dst,
            send_sem=send_sem,
            recv_sem=recv_sem,
            device_id={"ep": e, "tp": t},
            device_id_type=pl.DeviceIdType.MESH,
        )

    loads[7].wait()
    id0 = ids_v[0:1, :]
    id1 = ids_v[1:2, :]
    low = iota((n_ep, rows), 0) * local_experts
    high = low + local_experts
    hits = jnp.where(
        ((id0 >= low) & (id0 < high)) | ((id1 >= low) & (id1 < high)), 1.0, 0.0
    ).astype(F32)
    before = jnp.where(iota((rows, rows), 0) < iota((rows, rows), 1), 1.0, 0.0).astype(BF16)
    rank = dot(hits.astype(BF16), before)
    slot_of = jnp.where(hits > 0.5, rank, -1.0)
    slot_row = iota((slots, rows), 0).astype(F32)
    select = jnp.concatenate(
        [jnp.where(slot_row == slot_of[d : d + 1, :], 1.0, 0.0).astype(F32) for d in range(n_ep)],
        axis=0,
    )
    tag0 = jnp.sum(select * (id0.astype(F32) + 1.0), axis=1, keepdims=True)
    tag1 = jnp.sum(select * (id1.astype(F32) + 1.0), axis=1, keepdims=True)
    lane = iota((n_ep * slots, 128), 1)
    tags = jnp.where(lane == 0, tag0, jnp.where(lane == 1, tag1, 0.0))
    for d in range(n_ep):
        meta_send[d] = tags[d * slots : (d + 1) * slots]
    meta_recv[my_e] = meta_send[my_e]
    select_b = select.astype(BF16)

    for i in (0, 1, 2, 3, 4, 5, 6):
        loads[i].wait()
    resid = residual_v[...].astype(F32)
    gain = norm_gain_v[...].astype(F32).reshape(1, width)
    normed_all = (resid * inverse_rms(resid) * gain).astype(BF16)
    own = jnp.where(
        iota((seqs, rows), 1) == my_t * seqs + iota((seqs, rows), 0), 1.0, 0.0
    ).astype(BF16)
    normed = dot(own, normed_all).astype(BF16)
    latent_raw = dot(normed, latent_weight_v[...])
    new_latent = (
        latent_raw * inverse_rms(latent_raw) * latent_gain_v[...].astype(F32).reshape(1, latent)
    ).astype(BF16)
    position = jnp.zeros((seqs, 1), F32)
    for s in range(seqs):
        position = jnp.where(iota((seqs, 1), 0) == s, lengths[s].astype(F32), position)
    index = iota((1, rope_width), 1)
    index = jnp.where(index >= half, index - half, index).astype(F32)
    frequency = jnp.power(jnp.full((1, rope_width), ROPE_BASE, F32), -2.0 * index / rope_width)
    angles = position * frequency
    cosine = jnp.cos(angles)
    sine = jnp.sin(angles)
    weight_r = rope_weight_v[...]
    swapped = jnp.concatenate([-weight_r[half:], weight_r[:half]], axis=0)
    new_rope = (
        dot(normed, weight_r, ((1,), (1,))) * cosine + dot(normed, swapped, ((1,), (1,))) * sine
    ).astype(BF16)
    latent_out[...] = new_latent
    rope_out[...] = new_rope
    source = iota((rope_width, rope_width), 0)
    target = iota((rope_width, rope_width), 1)
    turn = (
        jnp.where(source + half == target, 1.0, 0.0) - jnp.where(source == target + half, 1.0, 0.0)
    ).astype(BF16)

    new_latent_f = new_latent.astype(F32)
    new_rope_f = new_rope.astype(F32)
    mixed_latents = []
    for s in range(seqs):
        query = query_v[s]
        query_r = query_rope_v[s]
        turned = (
            query_r.astype(F32) * cosine[s : s + 1] + dot(query_r, turn) * sine[s : s + 1]
        ).astype(BF16)
        fresh_latent = new_latent_f[s : s + 1]
        fresh = (
            jnp.sum(query.astype(F32) * fresh_latent, axis=1, keepdims=True)
            + jnp.sum(turned.astype(F32) * new_rope_f[s : s + 1], axis=1, keepdims=True)
        ) * scale
        ropes[s].wait()
        caches[s].wait()
        score = (dot(query, cache_v[s], ((1,), (1,))) + dot(turned, rope_v[s])) * scale
        score = jnp.where(iota((heads, length), 1) < lengths[s], score, -jnp.inf)
        top = jnp.maximum(jnp.max(score, axis=1, keepdims=True), fresh)
        powers = jnp.exp(score - top)
        fresh_power = jnp.exp(fresh - top)
        inverse = 1.0 / (jnp.sum(powers, axis=1, keepdims=True) + fresh_power)
        weight = (powers * inverse).astype(BF16)
        fresh_weight = (fresh_power * inverse).astype(BF16).astype(F32)
        mixed_latents.append(
            (dot(weight, cache_v[s]) + fresh_weight * fresh_latent).astype(BF16)
        )
    lhs = jnp.concatenate(mixed_latents, axis=0)

    loads[8].wait()
    for t in range(n_tp):
        found = dot(lhs, value_v[:, t * head_cols : (t + 1) * head_cols])
        head = iota((heads, head_cols), 0)
        column = iota((heads, head_cols), 1) + t * head_cols
        mine = (column >= head * value_dim) & (column < (head + 1) * value_dim)
        block = jnp.zeros((pad, head_cols), F32)
        for s in range(seqs):
            line = jnp.sum(
                jnp.where(mine, found[s * heads : (s + 1) * heads], 0.0), axis=0, keepdims=True
            )
            block = jnp.where(iota((pad, head_cols), 0) == s, line, block)
        head_send[t] = block
    pl.semaphore_wait(barrier, n_dev - 1)
    for i in range(1, n_tp):
        t = lax.rem(my_t + i, n_tp)
        remote(
            head_send.at[t], head_recv.at[my_t], head_sems.at[0, t], head_sems.at[1, my_t], my_e, t
        ).start()
    for i in range(1, n_ep):
        e = lax.rem(my_e + i, n_ep)
        remote(
            meta_send.at[e], meta_recv.at[my_e], meta_sems.at[0, e], meta_sems.at[1, my_e], e, my_t
        ).start()
    head_recv[my_t] = head_send[my_t]
    loads[9].wait()
    line = iota((rows, n_tp * pad), 0)
    spot = iota((rows, n_tp * pad), 1)
    inner = spot & (pad - 1)
    outer = lax.shift_right_logical(spot, pad.bit_length() - 1)
    gather = jnp.where((inner < seqs) & (line == outer * seqs + inner), 1.0, 0.0).astype(BF16)
    for i in range(1, n_tp):
        t = lax.rem(my_t + i, n_tp)
        remote(
            head_send.at[t], head_recv.at[t], head_sems.at[0, t], head_sems.at[1, t], my_e, t
        ).wait()
    by_heads = dot(
        gather, head_recv[...].reshape(n_tp * pad, head_cols).astype(BF16)
    ).astype(BF16)

    for i in range(1, n_tp + 1):
        t = lax.rem(my_t + i, n_tp)
        cols = pl.ds(pl.multiple_of(t * col, col), col)
        sum_send[t] = dot(by_heads, out_v[:, cols]).astype(BF16)
        if i < n_tp:
            remote(
                sum_send.at[t], sum_recv.at[my_t], sum_sems.at[0, t], sum_sems.at[1, my_t], my_e, t
            ).start()
    my_cols = pl.ds(pl.multiple_of(my_t * col, col), col)
    attended = sum_send[my_t].astype(F32)
    for i in range(1, n_tp):
        t = lax.rem(my_t + n_tp - i, n_tp)
        remote(
            sum_send.at[t], sum_recv.at[t], sum_sems.at[0, t], sum_sems.at[1, t], my_e, t
        ).wait()
        attended = attended + sum_recv[t].astype(F32)
    after = (residual_v[:, my_cols].astype(F32) + attended).astype(BF16)

    chosen = dot(select_b, after).astype(BF16)
    for d in range(n_ep):
        disp_send[d] = chosen[d * slots : (d + 1) * slots]
    disp_recv[my_e, my_t] = disp_send[my_e]

    def send_rows(i, carry):
        to = lax.rem(me + i, n_dev)
        e = to // n_tp
        t = lax.rem(to, n_tp)
        remote(
            disp_send.at[e],
            disp_recv.at[my_e, my_t],
            disp_sems.at[0, e, t],
            disp_sems.at[1, my_e, my_t],
            e,
            t,
        ).start()
        return carry

    lax.fori_loop(1, n_dev, send_rows, 0)
    for load in loads[10:13]:
        load.wait()

    def await_rows(i, carry):
        to = lax.rem(me + n_dev - i, n_dev)
        e = to // n_tp
        t = lax.rem(to, n_tp)
        remote(
            disp_send.at[e], disp_recv.at[e, t], disp_sems.at[0, e, t], disp_sems.at[1, e, t], e, t
        ).wait()
        return carry

    for i in range(1, n_ep):
        e = lax.rem(my_e + i, n_ep)
        remote(
            meta_send.at[e], meta_recv.at[e], meta_sems.at[0, e], meta_sems.at[1, e], e, my_t
        ).wait()
    lax.fori_loop(1, n_dev, await_rows, 0)
    total = n_ep * slots
    taken = jnp.concatenate(
        [disp_recv[:, t].reshape(total, col) for t in range(n_tp)], axis=1
    ).astype(F32)
    mixer = mixer_gain_v[...].astype(F32).reshape(1, width)
    expert_in = (taken * inverse_rms(taken) * mixer).astype(BF16)
    group_logits = dot(expert_in, group_router_v[...], ((1,), (1,)))
    expert_logits = dot(expert_in, expert_router_v[...], ((1,), (1,)))
    meta = meta_recv[...].reshape(total, 128)
    name0 = meta[:, 0:1] - 1.0
    name1 = meta[:, 1:2] - 1.0
    group_low = (iota((total, groups), 1) * per_group).astype(F32)
    in_group = (name0 >= group_low) & (name0 < group_low + per_group)
    group_top = jnp.sum(jnp.where(in_group, group_logits, 0.0), axis=1, keepdims=True)
    share = 1.0 / jnp.sum(jnp.exp(group_logits - group_top), axis=1, keepdims=True)
    number = iota((total, experts), 1).astype(F32)
    pick0 = jnp.sum(jnp.where(number == name0, expert_logits, 0.0), axis=1, keepdims=True)
    pick1 = jnp.sum(jnp.where(number == name1, expert_logits, 0.0), axis=1, keepdims=True)
    route0 = share / (1.0 + jnp.exp(pick1 - pick0))
    route1 = share / (1.0 + jnp.exp(pick0 - pick1))

    acts = []
    routes = []
    for l in range(local_experts):
        name = (my_e * local_experts + l).astype(F32)
        routes.append(
            jnp.where(name0 == name, route0, 0.0) + jnp.where(name1 == name, route1, 0.0)
        )
        expert_loads[0][l].wait()
        gate = dot(expert_in, gate_v[l])
        expert_loads[1][l].wait()
        up = dot(expert_in, up_v[l])
        acts.append((gate / (1.0 + jnp.exp(-gate)) * up).astype(BF16))
    for load in expert_loads[2]:
        load.wait()
    for i in range(1, n_tp + 1):
        t = lax.rem(my_t + i, n_tp)
        cols = pl.ds(pl.multiple_of(t * col, col), col)
        part = jnp.zeros((total, col), F32)
        for l in range(local_experts):
            part = part + routes[l] * dot(acts[l], down_v[l, :, cols])
        part = part.astype(BF16)
        for e in range(n_ep):
            ret_send[e, t] = part[e * slots : (e + 1) * slots]
        for k in range(1 if i == n_tp else 0, n_ep):
            e = lax.rem(my_e + k, n_ep)
            remote(
                ret_send.at[e, t],
                ret_recv.at[my_e, my_t],
                ret_sems.at[0, e, t],
                ret_sems.at[1, my_e, my_t],
                e,
                t,
            ).start()
    ret_recv[my_e, my_t] = ret_send[my_e, my_t]

    def await_sums(i, carry):
        to = lax.rem(me + n_dev - i, n_dev)
        e = to // n_tp
        t = lax.rem(to, n_tp)
        remote(
            ret_send.at[e, t], ret_recv.at[e, t], ret_sems.at[0, e, t], ret_sems.at[1, e, t], e, t
        ).wait()
        return carry

    lax.fori_loop(1, n_dev, await_sums, 0)
    gathered = ret_recv[:, 0].astype(F32)
    for t in range(1, n_tp):
        gathered = gathered + ret_recv[:, t].astype(F32)
    moe = dot(
        select, gathered.reshape(total, col), ((0,), (0,)), precision=lax.Precision.HIGHEST
    )
    share_send[...] = (after.astype(F32) + moe).astype(BF16)
    for i in range(1, n_tp):
        t = lax.rem(my_t + i, n_tp)
        remote(
            share_send, share_recv.at[my_t], share_sems.at[0, t], share_sems.at[1, my_t], my_e, t
        ).start()
    share_recv[my_t] = share_send[...]
    for i in range(1, n_tp):
        t = lax.rem(my_t + n_tp - i, n_tp)
        remote(
            share_send, share_recv.at[t], share_sems.at[0, t], share_sems.at[1, t], my_e, t
        ).wait()
    for t in range(n_tp):
        mixed_out[:, t * col : (t + 1) * col] = share_recv[t]


def on_device(n_ep, n_tp, *args):
    (
        residual,
        cache_latent,
        cache_rope,
        lengths,
        query_latent,
        query_rope,
        norm_gain,
        latent_weight,
        latent_gain,
        rope_weight,
        value_weight,
        out_weight,
        mixer_gain,
        group_router,
        expert_router,
        expert_ids,
        gate_weight,
        up_weight,
        down_weight,
    ) = args
    rows, width = residual.shape
    seqs, heads, latent = query_latent.shape
    rope_width = query_rope.shape[2]
    local_experts = gate_weight.shape[0]
    experts = expert_router.shape[1]
    per_group = experts // group_router.shape[1]
    capacity = 2 * rows * TOPK // experts
    slots = capacity if per_group == TOPK == local_experts else min(local_experts * capacity, rows)
    slots = -(-slots // 16) * 16
    col = width // n_tp
    head_cols = out_weight.shape[0]
    pad = 8
    while pad < seqs:
        pad *= 2
    value_dim = value_weight.shape[1] // heads
    scale = float((value_dim + rope_width) ** (-0.5))
    group_router = group_router.T
    expert_router = expert_router.T
    expert_ids = expert_ids.T
    hbm = pl.BlockSpec(memory_space=pl.ANY)
    vmem = pl.BlockSpec(memory_space=pltpu.VMEM)
    smem = pl.BlockSpec(memory_space=pltpu.SMEM)

    def held(array):
        return pltpu.VMEM(array.shape, array.dtype)

    dma = pltpu.SemaphoreType.DMA
    return pl.pallas_call(
        functools.partial(layer, (n_ep, n_tp, slots, scale)),
        out_shape=(
            jax.ShapeDtypeStruct((rows, width), BF16),
            jax.ShapeDtypeStruct((seqs, latent), BF16),
            jax.ShapeDtypeStruct((seqs, rope_width), BF16),
        ),
        in_specs=[hbm] * 3 + [smem] + [hbm] * 15,
        out_specs=(vmem, vmem, vmem),
        scratch_shapes=[
            held(residual),
            held(cache_latent),
            held(cache_rope),
            held(query_latent),
            held(query_rope),
            held(norm_gain),
            held(latent_weight),
            held(latent_gain),
            held(rope_weight),
            held(value_weight),
            held(out_weight),
            held(mixer_gain),
            held(group_router),
            held(expert_router),
            held(expert_ids),
            held(gate_weight),
            held(up_weight),
            held(down_weight),
            pltpu.VMEM((n_tp, pad, head_cols), F32),
            pltpu.VMEM((n_tp, pad, head_cols), F32),
            pltpu.VMEM((n_ep, slots, 128), F32),
            pltpu.VMEM((n_ep, slots, 128), F32),
            pltpu.VMEM((n_tp, rows, col), BF16),
            pltpu.VMEM((n_tp, rows, col), BF16),
            pltpu.VMEM((n_ep, slots, col), BF16),
            pltpu.VMEM((n_ep, n_tp, slots, col), BF16),
            pltpu.VMEM((n_ep, n_tp, slots, col), BF16),
            pltpu.VMEM((n_ep, n_tp, slots, col), BF16),
            pltpu.VMEM((rows, col), BF16),
            pltpu.VMEM((n_tp, rows, col), BF16),
            dma((13,)),
            dma((seqs,)),
            dma((seqs,)),
            dma((3, local_experts)),
            dma((2, n_tp)),
            dma((2, n_ep)),
            dma((2, n_tp)),
            dma((2, n_ep, n_tp)),
            dma((2, n_ep, n_tp)),
            dma((2, n_tp)),
        ],
        compiler_params=pltpu.CompilerParams(collective_id=0, has_side_effects=True),
        name="layer",
    )(
        residual,
        cache_latent,
        cache_rope,
        lengths,
        query_latent,
        query_rope,
        norm_gain,
        latent_weight,
        latent_gain,
        rope_weight,
        value_weight,
        out_weight,
        mixer_gain,
        group_router,
        expert_router,
        expert_ids,
        gate_weight,
        up_weight,
        down_weight,
    )


def solution(mesh):
    in_specs = (
        P("ep", None),
        P(("ep", "tp"), None, None),
        P(("ep", "tp"), None, None),
        P(("ep", "tp")),
        P(("ep", "tp"), None, None),
        P(("ep", "tp"), None, None),
        P(),
        P(),
        P(),
        P(),
        P(),
        P("tp", None),
        P(),
        P(),
        P(),
        P("ep", None),
        P("ep", None, "tp"),
        P("ep", None, "tp"),
        P("ep", "tp", None),
    )
    out_specs = (P("ep", None), P(("ep", "tp"), None), P(("ep", "tp"), None))
    return jax.shard_map(
        functools.partial(on_device, mesh.shape["ep"], mesh.shape["tp"]),
        mesh=mesh,
        in_specs=in_specs,
        out_specs=out_specs,
        check_vma=False,
    )
```

time: 178 us -> 52.8 us (0.30)
  waiting for transfers between devices: 93.9 us -> 0 us
  Pallas kernels: 0 us -> 47.9 us
  blocking collectives: 24.5 us -> 0 us
  matrix products: 21.4 us -> 0 us
  between operations: 14.3 us -> 0.65 us
  starting transfers between devices: 10.1 us -> 0 us
  other arithmetic: 7.81 us -> 0 us
    psum x1 -> x0, waiting for transfers between devices: 53.8 us -> none  [on_device(): attended = lax.psum(head_terms, 'tp')]
    pallas_call x0 -> x1, Pallas kernels: none -> 47.9 us  [on_device(): pl.pallas_call(functools.partial(layer, (n_ep, n_tp, slots, scale)), out_...]
    reduce_scatter x1 -> x0, waiting for transfers between devices: 30.9 us -> none  [on_device(): lax.psum_scatter(expert_terms, 'tp', scatter_dimension=3, tiled=True)]
    dot_general x15 -> x0, matrix products: 21.4 us -> none  [the longest x1 6.04 us: on_device(): jnp.einsum('secf,efd->secd', activation, down_weight, preferred_element_t...]
    all_gather x1 -> x0, blocking collectives: 14 us -> none  [on_device(): mixed = lax.all_gather(mixed_share, 'tp', axis=1, tiled=True)]
    all_to_all x1 -> x0, blocking collectives: 10.6 us -> none  [on_device(): lax.all_to_all(outbound, 'ep', split_axis=0, concat_axis=0, tiled=True)]
    all_to_all x2 -> x0, starting transfers between devices: 10 us -> none  [the longest x1 6.35 us: on_device(): lax.all_to_all(head_values, 'tp', split_axis=1, concat_axis=0, tiled=True)]
    all_to_all x2 -> x0, waiting for transfers between devices: 9.22 us -> none  [the longest x1 4.83 us: on_device(): lax.all_to_all(head_values, 'tp', split_axis=1, concat_axis=0, tiled=True)]
  transfers between devices with their start and end apart: 4 -> 0, of which waited for: 4 -> 0; matrix products, arithmetic and copies ran while one was open for 1% -> 0% of each run, Pallas kernels for 0% -> 0%
where the time goes in v1:
time: 52.8 us; the launch traced here: 52.6 us
  Pallas kernels  47.9 us (91%)
  local copies, waits for them, and re-layouts  4.05 us (8%)
  between operations  0.65 us (1%)
    pallas_call x1, Pallas kernels, on_device(): pl.pallas_call(functools.partial(layer, (n_ep, n_tp, slots, scale)), out_...  47.9 us
    unnamed x3, local copies, waits for them, and re-layouts  4.05 us

profile of v1, /device:TPU:0, one launch (start us, length us, event | category | flops | bytes accessed | tf_op | source)
XLA Modules:
  0.0 52.6 jit_solution(3721696546020622092)
XLA Ops:
  0.6 47.9 %layer.1 = (bf16[32,2048]{1,0:T(8,128)(2,1)}, bf16[4,256]{1,0:T(4,128)(2,1)}, bf16[4,32]{1,0:T(4,128)(2,1)}) custom-call(bf16[32,2048]{1,0:T(8,128)(2,1)} %residual.1, bf16[4,2048,256]{2,1,0:T(8,128)(2,1)} %cache_latent.1, bf16[4,32,2048]{2,1,0:T(8,128)(2,1)} %cache_rope.1, s32[4]{0:T(128)} %lengths.1, bf16[4,32,256]{2,1,0:T(8,128)(2,1)} %query_latent.1, ...), custom_call_target="tpu_custom_call" | custom-call | tf_op jit(solution)/shard_map/layer/pallas_call | solution.py:513
  48.5 1.6 %copy.25 = bf16[32,2048]{1,0:T(8,128)(2,1)} copy(bf16[32,2048]{1,0:T(8,128)(2,1)} %get-tuple-element.6) | data formatting | bytes 262144
  50.1 1.3 %copy.26 = bf16[4,256]{1,0:T(4,128)(2,1)} copy(bf16[4,256]{1,0:T(4,128)(2,1)} %get-tuple-element.7) | data formatting | bytes 4096
  51.4 1.2 %copy.27 = bf16[4,32]{1,0:T(4,128)(2,1)} copy(bf16[4,32]{1,0:T(4,128)(2,1)} %get-tuple-element.8) | data formatting | bytes 512

commit v2 on v1

--- a/solution.py
+++ b/solution.py
@@ -34,7 +34,7 @@
     residual,
     cache_latent,
     cache_rope,
-    lengths,
+    lengths_hbm,
     query_latent,
     query_rope,
     norm_gain,
@@ -53,6 +53,7 @@
     mixed_out,
     latent_out,
     rope_out,
+    lengths,
     residual_v,
     cache_v,
     rope_v,
@@ -75,27 +76,37 @@
     head_recv,
     meta_send,
     meta_recv,
+    half_send,
+    half_recv,
     sum_send,
     sum_recv,
     disp_send,
     disp_recv,
+    pair_send,
+    pair_recv,
     ret_send,
     ret_recv,
     share_send,
     share_recv,
+    latent_v,
+    rope_key_v,
+    length_sem,
     load_sem,
     cache_sem,
     rope_sem,
     expert_sem,
     head_sems,
     meta_sems,
+    half_sems,
     sum_sems,
     disp_sems,
+    pass_sems,
+    pair_sems,
     ret_sems,
     share_sems,
+    store_sem,
 ):
     n_ep, n_tp, slots, scale = sizes
-    n_dev = n_ep * n_tp
     rows, width = residual_v.shape
     seqs, heads, latent = query_v.shape
     rope_width = rope_weight_v.shape[0]
@@ -112,7 +123,12 @@
 
     my_e = lax.axis_index("ep")
     my_t = lax.axis_index("tp")
-    me = my_e * n_tp + my_t
+    n_z = n_tp // 2
+    my_z = my_t // 2
+    core = lax.rem(my_t, 2)
+    sibling = my_t + 1 - 2 * core
+    n_chip = n_ep * n_z
+    my_chip = my_e * n_z + my_z
 
     loads = [
         pltpu.make_async_copy(src, dst, load_sem.at[i])
@@ -151,6 +167,8 @@
             [(gate_weight, gate_v), (up_weight, up_v), (down_weight, down_v)]
         )
     ]
+    length_load = pltpu.make_async_copy(lengths_hbm, lengths, length_sem)
+    length_load.start()
     for load in loads[:8]:
         load.start()
     for s in range(seqs):
@@ -158,25 +176,25 @@
         caches[s].start()
     for load in loads[8:]:
         load.start()
-    for kind in expert_loads:
-        for load in kind:
-            load.start()
 
     barrier = pltpu.get_barrier_semaphore()
 
-    def device(t):
-        return {"ep": t // n_tp, "tp": lax.rem(t, n_tp)}
-
-    def greet(i, carry):
+    def greet(e, t):
         pl.semaphore_signal(
             barrier,
             inc=1,
-            device_id=device(lax.rem(me + i, n_dev)),
+            device_id={"ep": e, "tp": t},
             device_id_type=pl.DeviceIdType.MESH,
         )
+
+    def greet_core(i, carry):
+        to = lax.rem(my_chip + i, n_chip)
+        greet(to // n_z, 2 * lax.rem(to, n_z) + core)
         return carry
 
-    lax.fori_loop(1, n_dev, greet, 0)
+    lax.fori_loop(1, n_chip, greet_core, 0)
+    for k in range(n_z):
+        greet(my_e, 2 * k + 1 - core)
 
     def remote(src, dst, send_sem, recv_sem, e, t):
         return pltpu.make_async_remote_copy(
@@ -188,31 +206,9 @@
             device_id_type=pl.DeviceIdType.MESH,
         )
 
-    loads[7].wait()
-    id0 = ids_v[0:1, :]
-    id1 = ids_v[1:2, :]
-    low = iota((n_ep, rows), 0) * local_experts
-    high = low + local_experts
-    hits = jnp.where(
-        ((id0 >= low) & (id0 < high)) | ((id1 >= low) & (id1 < high)), 1.0, 0.0
-    ).astype(F32)
-    before = jnp.where(iota((rows, rows), 0) < iota((rows, rows), 1), 1.0, 0.0).astype(BF16)
-    rank = dot(hits.astype(BF16), before)
-    slot_of = jnp.where(hits > 0.5, rank, -1.0)
-    slot_row = iota((slots, rows), 0).astype(F32)
-    select = jnp.concatenate(
-        [jnp.where(slot_row == slot_of[d : d + 1, :], 1.0, 0.0).astype(F32) for d in range(n_ep)],
-        axis=0,
-    )
-    tag0 = jnp.sum(select * (id0.astype(F32) + 1.0), axis=1, keepdims=True)
-    tag1 = jnp.sum(select * (id1.astype(F32) + 1.0), axis=1, keepdims=True)
-    lane = iota((n_ep * slots, 128), 1)
-    tags = jnp.where(lane == 0, tag0, jnp.where(lane == 1, tag1, 0.0))
-    for d in range(n_ep):
-        meta_send[d] = tags[d * slots : (d + 1) * slots]
-    meta_recv[my_e] = meta_send[my_e]
-    select_b = select.astype(BF16)
-
+    length_load.wait()
+    ropes[0].wait()
+    caches[0].wait()
     for i in (0, 1, 2, 3, 4, 5, 6):
         loads[i].wait()
     resid = residual_v[...].astype(F32)
@@ -240,8 +236,14 @@
     new_rope = (
         dot(normed, weight_r, ((1,), (1,))) * cosine + dot(normed, swapped, ((1,), (1,))) * sine
     ).astype(BF16)
-    latent_out[...] = new_latent
-    rope_out[...] = new_rope
+    latent_v[...] = new_latent
+    rope_key_v[...] = new_rope
+    stores = [
+        pltpu.make_async_copy(latent_v, latent_out, store_sem.at[n_tp]),
+        pltpu.make_async_copy(rope_key_v, rope_out, store_sem.at[n_tp + 1]),
+    ]
+    for store in stores:
+        store.start()
     source = iota((rope_width, rope_width), 0)
     target = iota((rope_width, rope_width), 1)
     turn = (
@@ -250,31 +252,45 @@
 
     new_latent_f = new_latent.astype(F32)
     new_rope_f = new_rope.astype(F32)
-    mixed_latents = []
-    for s in range(seqs):
+
+    def scores(s):
         query = query_v[s]
         query_r = query_rope_v[s]
         turned = (
             query_r.astype(F32) * cosine[s : s + 1] + dot(query_r, turn) * sine[s : s + 1]
         ).astype(BF16)
-        fresh_latent = new_latent_f[s : s + 1]
         fresh = (
-            jnp.sum(query.astype(F32) * fresh_latent, axis=1, keepdims=True)
+            jnp.sum(query.astype(F32) * new_latent_f[s : s + 1], axis=1, keepdims=True)
             + jnp.sum(turned.astype(F32) * new_rope_f[s : s + 1], axis=1, keepdims=True)
         ) * scale
-        ropes[s].wait()
-        caches[s].wait()
         score = (dot(query, cache_v[s], ((1,), (1,))) + dot(turned, rope_v[s])) * scale
         score = jnp.where(iota((heads, length), 1) < lengths[s], score, -jnp.inf)
+        return score, fresh
+
+    def mix(s, score, fresh):
         top = jnp.maximum(jnp.max(score, axis=1, keepdims=True), fresh)
         powers = jnp.exp(score - top)
         fresh_power = jnp.exp(fresh - top)
         inverse = 1.0 / (jnp.sum(powers, axis=1, keepdims=True) + fresh_power)
         weight = (powers * inverse).astype(BF16)
         fresh_weight = (fresh_power * inverse).astype(BF16).astype(F32)
-        mixed_latents.append(
-            (dot(weight, cache_v[s]) + fresh_weight * fresh_latent).astype(BF16)
-        )
+        return (dot(weight, cache_v[s]) + fresh_weight * new_latent_f[s : s + 1]).astype(BF16)
+
+    mixed_latents = []
+    waiting = None
+    for s in range(seqs):
+        if s > 0:
+            ropes[s].wait()
+            caches[s].wait()
+        if s == seqs - 1:
+            for kind in expert_loads:
+                for load in kind:
+                    load.start()
+        found = scores(s)
+        if waiting is not None:
+            mixed_latents.append(mix(s - 1, *waiting))
+        waiting = found
+    mixed_latents.append(mix(seqs - 1, *waiting))
     lhs = jnp.concatenate(mixed_latents, axis=0)
 
     loads[8].wait()
@@ -289,13 +305,38 @@
                 jnp.where(mine, found[s * heads : (s + 1) * heads], 0.0), axis=0, keepdims=True
             )
             block = jnp.where(iota((pad, head_cols), 0) == s, line, block)
-        head_send[t] = block
-    pl.semaphore_wait(barrier, n_dev - 1)
+        head_send[t] = block.astype(BF16)
+    pl.semaphore_wait(barrier, n_chip - 1 + n_z)
     for i in range(1, n_tp):
         t = lax.rem(my_t + i, n_tp)
         remote(
             head_send.at[t], head_recv.at[my_t], head_sems.at[0, t], head_sems.at[1, my_t], my_e, t
         ).start()
+    loads[7].wait()
+    id0 = ids_v[0:1, :]
+    id1 = ids_v[1:2, :]
+    low = iota((n_ep, rows), 0) * local_experts
+    high = low + local_experts
+    hits = jnp.where(
+        ((id0 >= low) & (id0 < high)) | ((id1 >= low) & (id1 < high)), 1.0, 0.0
+    ).astype(F32)
+    before = jnp.where(iota((rows, rows), 0) < iota((rows, rows), 1), 1.0, 0.0).astype(BF16)
+    rank = dot(hits.astype(BF16), before)
+    slot_of = jnp.where(hits > 0.5, rank, -1.0)
+    slot_row = iota((slots, rows), 0).astype(F32)
+    select = jnp.concatenate(
+        [jnp.where(slot_row == slot_of[d : d + 1, :], 1.0, 0.0).astype(F32) for d in range(n_ep)],
+        axis=0,
+    )
+    tag0 = jnp.sum(select * (id0.astype(F32) + 1.0), axis=1, keepdims=True)
+    tag1 = jnp.sum(select * (id1.astype(F32) + 1.0), axis=1, keepdims=True)
+    lane = iota((n_ep * slots, 128), 1)
+    tags = jnp.where(lane == 0, tag0, jnp.where(lane == 1, tag1, 0.0))
+    for d in range(n_ep):
+        meta_send[d] = tags[d * slots : (d + 1) * slots]
+    meta_recv[my_e] = meta_send[my_e]
+    select_b = select.astype(BF16)
+
     for i in range(1, n_ep):
         e = lax.rem(my_e + i, n_ep)
         remote(
@@ -314,25 +355,42 @@
             head_send.at[t], head_recv.at[t], head_sems.at[0, t], head_sems.at[1, t], my_e, t
         ).wait()
     by_heads = dot(
-        gather, head_recv[...].reshape(n_tp * pad, head_cols).astype(BF16)
+        gather, head_recv[...].astype(F32).reshape(n_tp * pad, head_cols).astype(BF16)
     ).astype(BF16)
 
-    for i in range(1, n_tp + 1):
-        t = lax.rem(my_t + i, n_tp)
-        cols = pl.ds(pl.multiple_of(t * col, col), col)
-        sum_send[t] = dot(by_heads, out_v[:, cols]).astype(BF16)
-        if i < n_tp:
+    def half(send, recv, sems, k):
+        return remote(send.at[k], recv.at[k], sems.at[0, k], sems.at[1, k], my_e, sibling)
+
+    def columns(t):
+        return pl.ds(pl.multiple_of(t * col, col), col)
+
+    for i in range(1, n_z + 1):
+        k = lax.rem(my_z + i, n_z)
+        half_send[k] = dot(by_heads, out_v[:, columns(2 * k + 1 - core)]).astype(BF16)
+        half(half_send, half_recv, half_sems, k).start()
+    for i in range(1, n_z + 1):
+        k = lax.rem(my_z + i, n_z)
+        t = 2 * k + core
+        part = dot(by_heads, out_v[:, columns(t)])
+        half(half_send, half_recv, half_sems, k).wait()
+        attended = part + half_recv[k].astype(F32)
+        if i < n_z:
+            sum_send[k] = attended.astype(BF16)
             remote(
-                sum_send.at[t], sum_recv.at[my_t], sum_sems.at[0, t], sum_sems.at[1, my_t], my_e, t
+                sum_send.at[k], sum_recv.at[my_z], sum_sems.at[0, k], sum_sems.at[1, my_z], my_e, t
             ).start()
-    my_cols = pl.ds(pl.multiple_of(my_t * col, col), col)
-    attended = sum_send[my_t].astype(F32)
-    for i in range(1, n_tp):
-        t = lax.rem(my_t + n_tp - i, n_tp)
-        remote(
-            sum_send.at[t], sum_recv.at[t], sum_sems.at[0, t], sum_sems.at[1, t], my_e, t
+    my_cols = columns(my_t)
+    for i in range(1, n_z):
+        k = lax.rem(my_z + n_z - i, n_z)
+        remote(
+            sum_send.at[k],
+            sum_recv.at[k],
+            sum_sems.at[0, k],
+            sum_sems.at[1, k],
+            my_e,
+            2 * k + core,
         ).wait()
-        attended = attended + sum_recv[t].astype(F32)
+        attended = attended + sum_recv[k].astype(F32)
     after = (residual_v[:, my_cols].astype(F32) + attended).astype(BF16)
 
     chosen = dot(select_b, after).astype(BF16)
@@ -341,30 +399,59 @@
     disp_recv[my_e, my_t] = disp_send[my_e]
 
     def send_rows(i, carry):
-        to = lax.rem(me + i, n_dev)
-        e = to // n_tp
-        t = lax.rem(to, n_tp)
+        to = lax.rem(my_chip + i, n_chip)
+        e = to // n_z
+        k = lax.rem(to, n_z)
         remote(
             disp_send.at[e],
             disp_recv.at[my_e, my_t],
-            disp_sems.at[0, e, t],
-            disp_sems.at[1, my_e, my_t],
+            disp_sems.at[0, e, k],
+            disp_sems.at[1, my_e, my_z],
             e,
-            t,
+            2 * k + core,
         ).start()
         return carry
 
-    lax.fori_loop(1, n_dev, send_rows, 0)
+    lax.fori_loop(1, n_chip, send_rows, 0)
+    remote(
+        disp_send.at[my_e],
+        disp_recv.at[my_e, my_t],
+        pass_sems.at[0, my_e, my_z],
+        pass_sems.at[1, my_e, my_z],
+        my_e,
+        sibling,
+    ).start()
     for load in loads[10:13]:
         load.wait()
 
+    def pass_rows(e, k):
+        return remote(
+            disp_recv.at[e, 2 * k + core],
+            disp_recv.at[e, 2 * k + core],
+            pass_sems.at[0, e, k],
+            pass_sems.at[1, e, k],
+            my_e,
+            sibling,
+        )
+
     def await_rows(i, carry):
-        to = lax.rem(me + n_dev - i, n_dev)
-        e = to // n_tp
-        t = lax.rem(to, n_tp)
-        remote(
-            disp_send.at[e], disp_recv.at[e, t], disp_sems.at[0, e, t], disp_sems.at[1, e, t], e, t
+        to = lax.rem(my_chip + n_chip - i, n_chip)
+        e = to // n_z
+        k = lax.rem(to, n_z)
+        remote(
+            disp_send.at[e],
+            disp_recv.at[e, 2 * k + core],
+            disp_sems.at[0, e, k],
+            disp_sems.at[1, e, k],
+            e,
+            2 * k + core,
         ).wait()
+        pass_rows(e, k).start()
+        return carry
+
+    def await_passed(i, carry):
+        to = lax.rem(my_chip + n_chip - i, n_chip)
+        pass_rows(to // n_z, lax.rem(to, n_z)).wait()
         return carry
 
     for i in range(1, n_ep):
@@ -372,7 +459,8 @@
         remote(
             meta_send.at[e], meta_recv.at[e], meta_sems.at[0, e], meta_sems.at[1, e], e, my_t
         ).wait()
-    lax.fori_loop(1, n_dev, await_rows, 0)
+    lax.fori_loop(1, n_chip, await_rows, 0)
+    lax.fori_loop(0, n_chip, await_passed, 0)
     total = n_ep * slots
     taken = jnp.concatenate(
         [disp_recv[:, t].reshape(total, col) for t in range(n_tp)], axis=1
@@ -408,39 +496,53 @@
         acts.append((gate / (1.0 + jnp.exp(-gate)) * up).astype(BF16))
     for load in expert_loads[2]:
         load.wait()
-    for i in range(1, n_tp + 1):
-        t = lax.rem(my_t + i, n_tp)
-        cols = pl.ds(pl.multiple_of(t * col, col), col)
-        part = jnp.zeros((total, col), F32)
-        for l in range(local_experts):
-            part = part + routes[l] * dot(acts[l], down_v[l, :, cols])
-        part = part.astype(BF16)
+    def expert_part(t):
+        part = routes[0] * dot(acts[0], down_v[0, :, columns(t)])
+        for l in range(1, local_experts):
+            part = part + routes[l] * dot(acts[l], down_v[l, :, columns(t)])
+        return part
+
+    for i in range(1, n_z + 1):
+        k = lax.rem(my_z + i, n_z)
+        pair_send[k] = expert_part(2 * k + 1 - core).astype(BF16)
+        half(pair_send, pair_recv, pair_sems, k).start()
+    for i in range(1, n_z + 1):
+        k = lax.rem(my_z + i, n_z)
+        t = 2 * k + core
+        part = expert_part(t)
+        half(pair_send, pair_recv, pair_sems, k).wait()
+        part = (part + pair_recv[k].astype(F32)).astype(BF16)
         for e in range(n_ep):
-            ret_send[e, t] = part[e * slots : (e + 1) * slots]
-        for k in range(1 if i == n_tp else 0, n_ep):
-            e = lax.rem(my_e + k, n_ep)
+            ret_send[e, k] = part[e * slots : (e + 1) * slots]
+        for d in range(1 if i == n_z else 0, n_ep):
+            e = lax.rem(my_e + d, n_ep)
             remote(
-                ret_send.at[e, t],
-                ret_recv.at[my_e, my_t],
-                ret_sems.at[0, e, t],
-                ret_sems.at[1, my_e, my_t],
+                ret_send.at[e, k],
+                ret_recv.at[my_e, my_z],
+                ret_sems.at[0, e, k],
+                ret_sems.at[1, my_e, my_z],
                 e,
                 t,
             ).start()
-    ret_recv[my_e, my_t] = ret_send[my_e, my_t]
+    ret_recv[my_e, my_z] = ret_send[my_e, my_z]
 
     def await_sums(i, carry):
-        to = lax.rem(me + n_dev - i, n_dev)
-        e = to // n_tp
-        t = lax.rem(to, n_tp)
-        remote(
-            ret_send.at[e, t], ret_recv.at[e, t], ret_sems.at[0, e, t], ret_sems.at[1, e, t], e, t
+        to = lax.rem(my_chip + n_chip - i, n_chip)
+        e = to // n_z
+        k = lax.rem(to, n_z)
+        remote(
+            ret_send.at[e, k],
+            ret_recv.at[e, k],
+            ret_sems.at[0, e, k],
+            ret_sems.at[1, e, k],
+            e,
+            2 * k + core,
         ).wait()
         return carry
 
-    lax.fori_loop(1, n_dev, await_sums, 0)
+    lax.fori_loop(1, n_chip, await_sums, 0)
     gathered = ret_recv[:, 0].astype(F32)
-    for t in range(1, n_tp):
+    for t in range(1, n_z):
         gathered = gathered + ret_recv[:, t].astype(F32)
     moe = dot(
         select, gathered.reshape(total, col), ((0,), (0,)), precision=lax.Precision.HIGHEST
@@ -451,14 +553,36 @@
         remote(
             share_send, share_recv.at[my_t], share_sems.at[0, t], share_sems.at[1, my_t], my_e, t
         ).start()
-    share_recv[my_t] = share_send[...]
+
+    def store(src, t):
+        return pltpu.make_async_copy(src, mixed_out.at[:, columns(t)], store_sem.at[t])
+
+    store(share_send, my_t).start()
     for i in range(1, n_tp):
         t = lax.rem(my_t + n_tp - i, n_tp)
         remote(
             share_send, share_recv.at[t], share_sems.at[0, t], share_sems.at[1, t], my_e, t
         ).wait()
-    for t in range(n_tp):
-        mixed_out[:, t * col : (t + 1) * col] = share_recv[t]
+        store(share_recv.at[t], t).start()
+    for k in range(n_tp):
+        store(share_send, k).wait()
+    for copy in stores:
+        copy.wait()
+
+
+def place(arrays):
+    def kernel(*refs):
+        for src, dst in zip(refs[: len(arrays)], refs[len(arrays) :]):
+            dst[...] = src[...]
+
+    vmem = pl.BlockSpec(memory_space=pltpu.VMEM)
+    return pl.pallas_call(
+        kernel,
+        out_shape=tuple(jax.ShapeDtypeStruct(a.shape, a.dtype) for a in arrays),
+        in_specs=[vmem] * len(arrays),
+        out_specs=(vmem,) * len(arrays),
+        name="place",
+    )(*arrays)
 
 
 def on_device(n_ep, n_tp, *args):
@@ -493,6 +617,7 @@
     slots = capacity if per_group == TOPK == local_experts else min(local_experts * capacity, rows)
     slots = -(-slots // 16) * 16
     col = width // n_tp
+    n_z = n_tp // 2
     head_cols = out_weight.shape[0]
     pad = 8
     while pad < seqs:
@@ -503,23 +628,22 @@
     expert_router = expert_router.T
     expert_ids = expert_ids.T
     hbm = pl.BlockSpec(memory_space=pl.ANY)
-    vmem = pl.BlockSpec(memory_space=pltpu.VMEM)
-    smem = pl.BlockSpec(memory_space=pltpu.SMEM)
 
     def held(array):
         return pltpu.VMEM(array.shape, array.dtype)
 
     dma = pltpu.SemaphoreType.DMA
-    return pl.pallas_call(
+    outs = pl.pallas_call(
         functools.partial(layer, (n_ep, n_tp, slots, scale)),
         out_shape=(
             jax.ShapeDtypeStruct((rows, width), BF16),
             jax.ShapeDtypeStruct((seqs, latent), BF16),
             jax.ShapeDtypeStruct((seqs, rope_width), BF16),
         ),
-        in_specs=[hbm] * 3 + [smem] + [hbm] * 15,
-        out_specs=(vmem, vmem, vmem),
+        in_specs=[hbm] * 19,
+        out_specs=(hbm, hbm, hbm),
         scratch_shapes=[
+            pltpu.SMEM(lengths.shape, lengths.dtype),
             held(residual),
             held(cache_latent),
             held(cache_rope),
@@ -538,28 +662,39 @@
             held(gate_weight),
             held(up_weight),
             held(down_weight),
-            pltpu.VMEM((n_tp, pad, head_cols), F32),
-            pltpu.VMEM((n_tp, pad, head_cols), F32),
+            pltpu.VMEM((n_tp, pad, head_cols), BF16),
+            pltpu.VMEM((n_tp, pad, head_cols), BF16),
             pltpu.VMEM((n_ep, slots, 128), F32),
             pltpu.VMEM((n_ep, slots, 128), F32),
-            pltpu.VMEM((n_tp, rows, col), BF16),
-            pltpu.VMEM((n_tp, rows, col), BF16),
+            pltpu.VMEM((n_z, rows, col), BF16),
+            pltpu.VMEM((n_z, rows, col), BF16),
+            pltpu.VMEM((n_z, rows, col), BF16),
+            pltpu.VMEM((n_z, rows, col), BF16),
             pltpu.VMEM((n_ep, slots, col), BF16),
             pltpu.VMEM((n_ep, n_tp, slots, col), BF16),
-            pltpu.VMEM((n_ep, n_tp, slots, col), BF16),
-            pltpu.VMEM((n_ep, n_tp, slots, col), BF16),
+            pltpu.VMEM((n_z, n_ep * slots, col), BF16),
+            pltpu.VMEM((n_z, n_ep * slots, col), BF16),
+            pltpu.VMEM((n_ep, n_z, slots, col), BF16),
+            pltpu.VMEM((n_ep, n_z, slots, col), BF16),
             pltpu.VMEM((rows, col), BF16),
             pltpu.VMEM((n_tp, rows, col), BF16),
+            pltpu.VMEM((seqs, latent), BF16),
+            pltpu.VMEM((seqs, rope_width), BF16),
+            dma,
             dma((13,)),
             dma((seqs,)),
             dma((seqs,)),
             dma((3, local_experts)),
             dma((2, n_tp)),
             dma((2, n_ep)),
+            dma((2, n_z)),
+            dma((2, n_z)),
+            dma((2, n_ep, n_z)),
+            dma((2, n_ep, n_z)),
+            dma((2, n_z)),
+            dma((2, n_ep, n_z)),
             dma((2, n_tp)),
-            dma((2, n_ep, n_tp)),
-            dma((2, n_ep, n_tp)),
-            dma((2, n_tp)),
+            dma((n_tp + 2,)),
         ],
         compiler_params=pltpu.CompilerParams(collective_id=0, has_side_effects=True),
         name="layer",
@@ -584,6 +719,7 @@
         up_weight,
         down_weight,
     )
+    return place(outs)
 
 
 def solution(mesh):

time: 52.8 us -> 43.5 us (0.82)
  Pallas kernels: 47.9 us -> 42.7 us
  local copies, waits for them, and re-layouts: 4.05 us -> 0 us
    pallas_call x1, Pallas kernels: 47.9 us -> 41.1 us  [on_device(): pl.pallas_call(functools.partial(layer, (n_ep, n_tp, slots, scale)), out_...]
    unnamed x3 -> x0, local copies, waits for them, and re-layouts: 4.05 us -> none
    pallas_call x0 -> x1, Pallas kernels: none -> 1.58 us  [place(): pl.pallas_call(kernel, out_shape=tuple((jax.ShapeDtypeStruct(a.shape, a.d...]
where the time goes in v2:
time: 43.5 us; the launch traced here: 43.4 us
  Pallas kernels  42.7 us (98%)
  between operations  0.65 us (1%)
    pallas_call x1, Pallas kernels, on_device(): pl.pallas_call(functools.partial(layer, (n_ep, n_tp, slots, scale)), out_...  41.1 us
    pallas_call x1, Pallas kernels, place(): pl.pallas_call(kernel, out_shape=tuple((jax.ShapeDtypeStruct(a.shape, a.d...  1.58 us

profile of v2, /device:TPU:0, one launch (start us, length us, event | category | flops | bytes accessed | tf_op | source)
XLA Modules:
  0.0 43.4 jit_solution(2396312893911561348)
XLA Ops:
  0.6 41.1 %layer.1 = (bf16[32,2048]{1,0:T(8,128)(2,1)}, bf16[4,256]{1,0:T(4,128)(2,1)}, bf16[4,32]{1,0:T(4,128)(2,1)}) custom-call(bf16[32,2048]{1,0:T(8,128)(2,1)} %residual.1, bf16[4,2048,256]{2,1,0:T(8,128)(2,1)} %cache_latent.1, bf16[4,32,2048]{2,1,0:T(8,128)(2,1)} %cache_rope.1, s32[4]{0:T(128)} %lengths_hbm.1, bf16[4,32,256]{2,1,0:T(8,128)(2,1)} %query_latent.1, ...), custom_call_target="tpu_custom_call" | custom-call | tf_op jit(solution)/shard_map/layer/pallas_call | solution.py:636
  41.8 1.6 %place.1 = (bf16[32,2048]{1,0:T(8,128)(2,1)}, bf16[4,256]{1,0:T(4,128)(2,1)}, bf16[4,32]{1,0:T(4,128)(2,1)}) custom-call(bf16[32,2048]{1,0:T(8,128)(2,1)} %get-tuple-element.6.refs_0_, bf16[4,256]{1,0:T(4,128)(2,1)} %get-tuple-element.7.refs_1_, bf16[4,32]{1,0:T(4,128)(2,1)} %get-tuple-element.8.refs_2_), custom_call_target="tpu_custom_call" | custom-call | tf_op jit(solution)/shard_map/place/pallas_call | solution.py:579

commit v3 on v2

--- a/solution.py
+++ b/solution.py
@@ -87,9 +87,7 @@
     ret_send,
     ret_recv,
     share_send,
-    share_recv,
-    latent_v,
-    rope_key_v,
+    gain_row,
     length_sem,
     load_sem,
     cache_sem,
@@ -169,15 +167,30 @@
     ]
     length_load = pltpu.make_async_copy(lengths_hbm, lengths, length_sem)
     length_load.start()
-    for load in loads[:8]:
-        load.start()
+    for i in (5, 6):
+        loads[i].start()
     for s in range(seqs):
         ropes[s].start()
         caches[s].start()
-    for load in loads[8:]:
+        if s == 0:
+            for i in (0, 1, 2, 3, 4):
+                loads[i].start()
+    for load in loads[7:]:
         load.start()
 
     barrier = pltpu.get_barrier_semaphore()
+
+    def flip(index, by, count):
+        found = 0
+        bit = 1
+        while bit < count:
+            found = found + bit * lax.rem(index // bit + by // bit, 2)
+            bit *= 2
+        return found
+
+    near_z = [flip(my_z, i, n_z) for i in range(n_z)]
+    near_e = [flip(my_e, i, n_ep) for i in range(n_ep)]
+    far_first = near_z[::-1]
 
     def greet(e, t):
         pl.semaphore_signal(
@@ -207,9 +220,38 @@
         )
 
     length_load.wait()
+    position = jnp.zeros((seqs, 1), F32)
+    for s in range(seqs):
+        position = jnp.where(iota((seqs, 1), 0) == s, lengths[s].astype(F32), position)
+    index = iota((1, rope_width), 1)
+    index = jnp.where(index >= half, index - half, index).astype(F32)
+    frequency = jnp.power(jnp.full((1, rope_width), ROPE_BASE, F32), -2.0 * index / rope_width)
+    angles = position * frequency
+    cosine = jnp.cos(angles)
+    sine = jnp.sin(angles)
+    source = iota((rope_width, rope_width), 0)
+    target = iota((rope_width, rope_width), 1)
+    turn = (
+        jnp.where(source + half == target, 1.0, 0.0) - jnp.where(source == target + half, 1.0, 0.0)
+    ).astype(BF16)
+
+
+    def scores(s):
+        query_r = query_rope_v[s]
+        turned = (
+            query_r.astype(F32) * cosine[s : s + 1] + dot(query_r, turn) * sine[s : s + 1]
+        ).astype(BF16)
+        score = (dot(query_v[s], cache_v[s], ((1,), (1,))) + dot(turned, rope_v[s])) * scale
+        score = jnp.where(iota((heads, length), 1) < lengths[s], score, -jnp.inf)
+        return score, turned
+
+    for i in (5, 6):
+        loads[i].wait()
     ropes[0].wait()
     caches[0].wait()
-    for i in (0, 1, 2, 3, 4, 5, 6):
+    waiting = scores(0)
+
+    for i in (0, 1, 2, 3, 4):
         loads[i].wait()
     resid = residual_v[...].astype(F32)
     gain = norm_gain_v[...].astype(F32).reshape(1, width)
@@ -222,73 +264,39 @@
     new_latent = (
         latent_raw * inverse_rms(latent_raw) * latent_gain_v[...].astype(F32).reshape(1, latent)
     ).astype(BF16)
-    position = jnp.zeros((seqs, 1), F32)
-    for s in range(seqs):
-        position = jnp.where(iota((seqs, 1), 0) == s, lengths[s].astype(F32), position)
-    index = iota((1, rope_width), 1)
-    index = jnp.where(index >= half, index - half, index).astype(F32)
-    frequency = jnp.power(jnp.full((1, rope_width), ROPE_BASE, F32), -2.0 * index / rope_width)
-    angles = position * frequency
-    cosine = jnp.cos(angles)
-    sine = jnp.sin(angles)
     weight_r = rope_weight_v[...]
     swapped = jnp.concatenate([-weight_r[half:], weight_r[:half]], axis=0)
     new_rope = (
         dot(normed, weight_r, ((1,), (1,))) * cosine + dot(normed, swapped, ((1,), (1,))) * sine
     ).astype(BF16)
-    latent_v[...] = new_latent
-    rope_key_v[...] = new_rope
-    stores = [
-        pltpu.make_async_copy(latent_v, latent_out, store_sem.at[n_tp]),
-        pltpu.make_async_copy(rope_key_v, rope_out, store_sem.at[n_tp + 1]),
-    ]
-    for store in stores:
-        store.start()
-    source = iota((rope_width, rope_width), 0)
-    target = iota((rope_width, rope_width), 1)
-    turn = (
-        jnp.where(source + half == target, 1.0, 0.0) - jnp.where(source == target + half, 1.0, 0.0)
-    ).astype(BF16)
-
+    latent_out[...] = new_latent
+    rope_out[...] = new_rope
     new_latent_f = new_latent.astype(F32)
     new_rope_f = new_rope.astype(F32)
 
-    def scores(s):
-        query = query_v[s]
-        query_r = query_rope_v[s]
-        turned = (
-            query_r.astype(F32) * cosine[s : s + 1] + dot(query_r, turn) * sine[s : s + 1]
-        ).astype(BF16)
+    def mix(s, score, turned):
         fresh = (
-            jnp.sum(query.astype(F32) * new_latent_f[s : s + 1], axis=1, keepdims=True)
+            jnp.sum(query_v[s].astype(F32) * new_latent_f[s : s + 1], axis=1, keepdims=True)
             + jnp.sum(turned.astype(F32) * new_rope_f[s : s + 1], axis=1, keepdims=True)
         ) * scale
-        score = (dot(query, cache_v[s], ((1,), (1,))) + dot(turned, rope_v[s])) * scale
-        score = jnp.where(iota((heads, length), 1) < lengths[s], score, -jnp.inf)
-        return score, fresh
-
-    def mix(s, score, fresh):
         top = jnp.maximum(jnp.max(score, axis=1, keepdims=True), fresh)
         powers = jnp.exp(score - top)
         fresh_power = jnp.exp(fresh - top)
         inverse = 1.0 / (jnp.sum(powers, axis=1, keepdims=True) + fresh_power)
-        weight = (powers * inverse).astype(BF16)
-        fresh_weight = (fresh_power * inverse).astype(BF16).astype(F32)
-        return (dot(weight, cache_v[s]) + fresh_weight * new_latent_f[s : s + 1]).astype(BF16)
+        fresh_weight = fresh_power.astype(BF16).astype(F32)
+        mixed = dot(powers.astype(BF16), cache_v[s]) + fresh_weight * new_latent_f[s : s + 1]
+        return (mixed * inverse).astype(BF16)
 
     mixed_latents = []
-    waiting = None
-    for s in range(seqs):
-        if s > 0:
-            ropes[s].wait()
-            caches[s].wait()
+    for s in range(1, seqs):
+        ropes[s].wait()
+        caches[s].wait()
         if s == seqs - 1:
             for kind in expert_loads:
                 for load in kind:
                     load.start()
         found = scores(s)
-        if waiting is not None:
-            mixed_latents.append(mix(s - 1, *waiting))
+        mixed_latents.append(mix(s - 1, *waiting))
         waiting = found
     mixed_latents.append(mix(seqs - 1, *waiting))
     lhs = jnp.concatenate(mixed_latents, axis=0)
@@ -307,8 +315,8 @@
             block = jnp.where(iota((pad, head_cols), 0) == s, line, block)
         head_send[t] = block.astype(BF16)
     pl.semaphore_wait(barrier, n_chip - 1 + n_z)
-    for i in range(1, n_tp):
-        t = lax.rem(my_t + i, n_tp)
+    for i in reversed(range(1, n_tp)):
+        t = flip(my_t, i, n_tp)
         remote(
             head_send.at[t], head_recv.at[my_t], head_sems.at[0, t], head_sems.at[1, my_t], my_e, t
         ).start()
@@ -364,24 +372,25 @@
     def columns(t):
         return pl.ds(pl.multiple_of(t * col, col), col)
 
-    for i in range(1, n_z + 1):
-        k = lax.rem(my_z + i, n_z)
+    for k in far_first:
         half_send[k] = dot(by_heads, out_v[:, columns(2 * k + 1 - core)]).astype(BF16)
         half(half_send, half_recv, half_sems, k).start()
-    for i in range(1, n_z + 1):
-        k = lax.rem(my_z + i, n_z)
-        t = 2 * k + core
-        part = dot(by_heads, out_v[:, columns(t)])
+    parts = [dot(by_heads, out_v[:, columns(2 * k + core)]) for k in far_first]
+    for i, k in enumerate(far_first):
         half(half_send, half_recv, half_sems, k).wait()
-        attended = part + half_recv[k].astype(F32)
-        if i < n_z:
+        attended = parts[i] + half_recv[k].astype(F32)
+        if i < n_z - 1:
             sum_send[k] = attended.astype(BF16)
             remote(
-                sum_send.at[k], sum_recv.at[my_z], sum_sems.at[0, k], sum_sems.at[1, my_z], my_e, t
+                sum_send.at[k],
+                sum_recv.at[my_z],
+                sum_sems.at[0, k],
+                sum_sems.at[1, my_z],
+                my_e,
+                2 * k + core,
             ).start()
     my_cols = columns(my_t)
-    for i in range(1, n_z):
-        k = lax.rem(my_z + n_z - i, n_z)
+    for k in reversed(far_first[:-1]):
         remote(
             sum_send.at[k],
             sum_recv.at[k],
@@ -398,21 +407,18 @@
         disp_send[d] = chosen[d * slots : (d + 1) * slots]
     disp_recv[my_e, my_t] = disp_send[my_e]
 
-    def send_rows(i, carry):
-        to = lax.rem(my_chip + i, n_chip)
-        e = to // n_z
-        k = lax.rem(to, n_z)
-        remote(
-            disp_send.at[e],
-            disp_recv.at[my_e, my_t],
-            disp_sems.at[0, e, k],
-            disp_sems.at[1, my_e, my_z],
-            e,
-            2 * k + core,
-        ).start()
-        return carry
-
-    lax.fori_loop(1, n_chip, send_rows, 0)
+    for i in reversed(range(n_z)):
+        for d in reversed(range(n_ep)):
+            if i + d > 0:
+                e, k = near_e[d], near_z[i]
+                remote(
+                    disp_send.at[e],
+                    disp_recv.at[my_e, my_t],
+                    disp_sems.at[0, e, k],
+                    disp_sems.at[1, my_e, my_z],
+                    e,
+                    2 * k + core,
+                ).start()
     remote(
         disp_send.at[my_e],
         disp_recv.at[my_e, my_t],
@@ -434,41 +440,57 @@
             sibling,
         )
 
-    def await_rows(i, carry):
-        to = lax.rem(my_chip + n_chip - i, n_chip)
-        e = to // n_z
-        k = lax.rem(to, n_z)
-        remote(
-            disp_send.at[e],
-            disp_recv.at[e, 2 * k + core],
-            disp_sems.at[0, e, k],
-            disp_sems.at[1, e, k],
-            e,
-            2 * k + core,
-        ).wait()
-        pass_rows(e, k).start()
-        return carry
-
-    def await_passed(i, carry):
-        to = lax.rem(my_chip + n_chip - i, n_chip)
-        pass_rows(to // n_z, lax.rem(to, n_z)).wait()
-        return carry
+    def await_rows(i):
+        for d in range(n_ep):
+            if i + d > 0:
+                e, k = near_e[d], near_z[i]
+                remote(
+                    disp_send.at[e],
+                    disp_recv.at[e, 2 * k + core],
+                    disp_sems.at[0, e, k],
+                    disp_sems.at[1, e, k],
+                    e,
+                    2 * k + core,
+                ).wait()
+                pass_rows(e, k).start()
 
     for i in range(1, n_ep):
-        e = lax.rem(my_e + i, n_ep)
+        e = near_e[i]
         remote(
             meta_send.at[e], meta_recv.at[e], meta_sems.at[0, e], meta_sems.at[1, e], e, my_t
         ).wait()
-    lax.fori_loop(1, n_chip, await_rows, 0)
-    lax.fori_loop(0, n_chip, await_passed, 0)
+    for kind in expert_loads:
+        for load in kind:
+            load.wait()
+    gain_row[...] = mixer_gain_v[...].astype(F32).reshape(1, width)
     total = n_ep * slots
-    taken = jnp.concatenate(
-        [disp_recv[:, t].reshape(total, col) for t in range(n_tp)], axis=1
-    ).astype(F32)
-    mixer = mixer_gain_v[...].astype(F32).reshape(1, width)
-    expert_in = (taken * inverse_rms(taken) * mixer).astype(BF16)
-    group_logits = dot(expert_in, group_router_v[...], ((1,), (1,)))
-    expert_logits = dot(expert_in, expert_router_v[...], ((1,), (1,)))
+    squares = jnp.zeros((total, 1), F32)
+    group_logits = jnp.zeros((total, groups), F32)
+    expert_logits = jnp.zeros((total, experts), F32)
+    gates = [jnp.zeros((total, gate_v.shape[2]), F32) for _ in range(local_experts)]
+    ups = [jnp.zeros((total, gate_v.shape[2]), F32) for _ in range(local_experts)]
+    await_rows(0)
+    for i in range(n_z):
+        if i + 1 < n_z:
+            await_rows(i + 1)
+        k = near_z[i]
+        for d in range(n_ep):
+            pass_rows(near_e[d], k).wait()
+        span = pl.ds(pl.multiple_of(2 * k * col, 2 * col), 2 * col)
+        taken = jnp.concatenate(
+            [disp_recv[:, 2 * k + h].reshape(total, col) for h in range(2)], axis=1
+        ).astype(F32)
+        squares = squares + jnp.sum(taken * taken, axis=1, keepdims=True)
+        mixer = gain_row[:, span]
+        scaled = (taken * mixer).astype(BF16)
+        for l in range(local_experts):
+            gates[l] = gates[l] + dot(scaled, gate_v[l, span, :])
+            ups[l] = ups[l] + dot(scaled, up_v[l, span, :])
+        group_logits = group_logits + dot(scaled, group_router_v[:, span], ((1,), (1,)))
+        expert_logits = expert_logits + dot(scaled, expert_router_v[:, span], ((1,), (1,)))
+    factor = lax.rsqrt(squares / width + NORM_EPSILON)
+    group_logits = group_logits * factor
+    expert_logits = expert_logits * factor
     meta = meta_recv[...].reshape(total, 128)
     name0 = meta[:, 0:1] - 1.0
     name1 = meta[:, 1:2] - 1.0
@@ -489,33 +511,26 @@
         routes.append(
             jnp.where(name0 == name, route0, 0.0) + jnp.where(name1 == name, route1, 0.0)
         )
-        expert_loads[0][l].wait()
-        gate = dot(expert_in, gate_v[l])
-        expert_loads[1][l].wait()
-        up = dot(expert_in, up_v[l])
-        acts.append((gate / (1.0 + jnp.exp(-gate)) * up).astype(BF16))
-    for load in expert_loads[2]:
-        load.wait()
+        gate = gates[l] * factor
+        acts.append((gate / (1.0 + jnp.exp(-gate)) * (ups[l] * factor)).astype(BF16))
     def expert_part(t):
         part = routes[0] * dot(acts[0], down_v[0, :, columns(t)])
         for l in range(1, local_experts):
             part = part + routes[l] * dot(acts[l], down_v[l, :, columns(t)])
         return part
 
-    for i in range(1, n_z + 1):
-        k = lax.rem(my_z + i, n_z)
+    for k in far_first:
         pair_send[k] = expert_part(2 * k + 1 - core).astype(BF16)
         half(pair_send, pair_recv, pair_sems, k).start()
-    for i in range(1, n_z + 1):
-        k = lax.rem(my_z + i, n_z)
+    for i, k in enumerate(far_first):
         t = 2 * k + core
         part = expert_part(t)
         half(pair_send, pair_recv, pair_sems, k).wait()
         part = (part + pair_recv[k].astype(F32)).astype(BF16)
         for e in range(n_ep):
             ret_send[e, k] = part[e * slots : (e + 1) * slots]
-        for d in range(1 if i == n_z else 0, n_ep):
-            e = lax.rem(my_e + d, n_ep)
+        for d in reversed(range(1 if i == n_z - 1 else 0, n_ep)):
+            e = near_e[d]
             remote(
                 ret_send.at[e, k],
                 ret_recv.at[my_e, my_z],
@@ -526,61 +541,70 @@
             ).start()
     ret_recv[my_e, my_z] = ret_send[my_e, my_z]
 
-    def await_sums(i, carry):
-        to = lax.rem(my_chip + n_chip - i, n_chip)
-        e = to // n_z
-        k = lax.rem(to, n_z)
-        remote(
-            ret_send.at[e, k],
-            ret_recv.at[e, k],
-            ret_sems.at[0, e, k],
-            ret_sems.at[1, e, k],
-            e,
-            2 * k + core,
-        ).wait()
-        return carry
-
-    lax.fori_loop(1, n_chip, await_sums, 0)
+    for i in range(n_z):
+        for d in range(n_ep):
+            if i + d > 0:
+                e, k = near_e[d], near_z[i]
+                remote(
+                    ret_send.at[e, k],
+                    ret_recv.at[e, k],
+                    ret_sems.at[0, e, k],
+                    ret_sems.at[1, e, k],
+                    e,
+                    2 * k + core,
+                ).wait()
     gathered = ret_recv[:, 0].astype(F32)
     for t in range(1, n_z):
         gathered = gathered + ret_recv[:, t].astype(F32)
-    moe = dot(
-        select, gathered.reshape(total, col), ((0,), (0,)), precision=lax.Precision.HIGHEST
-    )
+    gathered = gathered.reshape(total, col)
+    coarse = gathered.astype(BF16)
+    fine = (gathered - coarse.astype(F32)).astype(BF16)
+    moe = dot(select_b, coarse, ((0,), (0,))) + dot(select_b, fine, ((0,), (0,)))
     share_send[...] = (after.astype(F32) + moe).astype(BF16)
+    own_store = pltpu.make_async_copy(share_send, mixed_out.at[:, my_cols], store_sem)
+    for i in reversed(range(1, n_tp)):
+        t = flip(my_t, i, n_tp)
+        remote(
+            share_send,
+            mixed_out.at[:, my_cols],
+            share_sems.at[0, t],
+            share_sems.at[1, my_t],
+            my_e,
+            t,
+        ).start()
+    own_store.start()
     for i in range(1, n_tp):
-        t = lax.rem(my_t + i, n_tp)
+        t = flip(my_t, i, n_tp)
         remote(
-            share_send, share_recv.at[my_t], share_sems.at[0, t], share_sems.at[1, my_t], my_e, t
-        ).start()
-
-    def store(src, t):
-        return pltpu.make_async_copy(src, mixed_out.at[:, columns(t)], store_sem.at[t])
-
-    store(share_send, my_t).start()
-    for i in range(1, n_tp):
-        t = lax.rem(my_t + n_tp - i, n_tp)
-        remote(
-            share_send, share_recv.at[t], share_sems.at[0, t], share_sems.at[1, t], my_e, t
+            share_send,
+            mixed_out.at[:, columns(t)],
+            share_sems.at[0, t],
+            share_sems.at[1, t],
+            my_e,
+            t,
         ).wait()
-        store(share_recv.at[t], t).start()
-    for k in range(n_tp):
-        store(share_send, k).wait()
-    for copy in stores:
-        copy.wait()
+    own_store.wait()
 
 
 def place(arrays):
+    count = len(arrays)
+
     def kernel(*refs):
-        for src, dst in zip(refs[: len(arrays)], refs[len(arrays) :]):
-            dst[...] = src[...]
-
-    vmem = pl.BlockSpec(memory_space=pltpu.VMEM)
+        copies = [
+            pltpu.make_async_copy(refs[i], refs[count + i], refs[-1].at[i]) for i in range(count)
+        ]
+        for copy in copies:
+            copy.start()
+        for copy in copies:
+            copy.wait()
+
+    arrays = [pltpu.with_memory_space_constraint(a, pltpu.VMEM) for a in arrays]
     return pl.pallas_call(
         kernel,
         out_shape=tuple(jax.ShapeDtypeStruct(a.shape, a.dtype) for a in arrays),
-        in_specs=[vmem] * len(arrays),
-        out_specs=(vmem,) * len(arrays),
+        in_specs=[pl.BlockSpec(memory_space=pltpu.VMEM)] * count,
+        out_specs=(pl.BlockSpec(memory_space=pl.ANY),) * count,
+        scratch_shapes=[pltpu.SemaphoreType.DMA((count,))],
         name="place",
     )(*arrays)
 
@@ -636,12 +660,12 @@
     outs = pl.pallas_call(
         functools.partial(layer, (n_ep, n_tp, slots, scale)),
         out_shape=(
-            jax.ShapeDtypeStruct((rows, width), BF16),
-            jax.ShapeDtypeStruct((seqs, latent), BF16),
-            jax.ShapeDtypeStruct((seqs, rope_width), BF16),
+            pltpu.VMEM((rows, width), BF16),
+            pltpu.VMEM((seqs, latent), BF16),
+            pltpu.VMEM((seqs, rope_width), BF16),
         ),
         in_specs=[hbm] * 19,
-        out_specs=(hbm, hbm, hbm),
+        out_specs=(pl.BlockSpec(memory_space=pltpu.VMEM),) * 3,
         scratch_shapes=[
             pltpu.SMEM(lengths.shape, lengths.dtype),
             held(residual),
@@ -677,9 +701,7 @@
             pltpu.VMEM((n_ep, n_z, slots, col), BF16),
             pltpu.VMEM((n_ep, n_z, slots, col), BF16),
             pltpu.VMEM((rows, col), BF16),
-            pltpu.VMEM((n_tp, rows, col), BF16),
-            pltpu.VMEM((seqs, latent), BF16),
-            pltpu.VMEM((seqs, rope_width), BF16),
+            pltpu.VMEM((1, width), F32),
             dma,
             dma((13,)),
             dma((seqs,)),
@@ -694,7 +716,7 @@
             dma((2, n_z)),
             dma((2, n_ep, n_z)),
             dma((2, n_tp)),
-            dma((n_tp + 2,)),
+            dma,
         ],
         compiler_params=pltpu.CompilerParams(collective_id=0, has_side_effects=True),
         name="layer",

time: 43.5 us -> 41.3 us (0.949)
  Pallas kernels: 42.7 us -> 40.5 us
    pallas_call x1, Pallas kernels: 41.1 us -> 39.8 us  [on_device(): pl.pallas_call(functools.partial(layer, (n_ep, n_tp, slots, scale)), out_...]
    pallas_call x1, Pallas kernels: 1.58 us -> 0.69 us  [place(): pl.pallas_call(kernel, out_shape=tuple((jax.ShapeDtypeStruct(a.shape, a.d...]
where the time goes in v3:
time: 41.3 us; the launch traced here: 41.1 us
  Pallas kernels  40.5 us (98%)
  between operations  0.65 us (2%)
    pallas_call x1, Pallas kernels, on_device(): pl.pallas_call(functools.partial(layer, (n_ep, n_tp, slots, scale)), out_...  39.8 us

profile of v3, /device:TPU:0, one launch (start us, length us, event | category | flops | bytes accessed | tf_op | source)
XLA Modules:
  0.0 41.1 jit_solution(5182882316638162234)
XLA Ops:
  0.6 39.8 %layer.1 = (bf16[32,2048]{1,0:T(8,128)(2,1)S(1)}, bf16[4,256]{1,0:T(4,128)(2,1)S(1)}, bf16[4,32]{1,0:T(4,128)(2,1)S(1)}) custom-call(bf16[32,2048]{1,0:T(8,128)(2,1)} %residual.1, bf16[4,2048,256]{2,1,0:T(8,128)(2,1)} %cache_latent.1, bf16[4,32,2048]{2,1,0:T(8,128)(2,1)} %cache_rope.1, s32[4]{0:T(128)} %lengths_hbm.1, bf16[4,32,256]{2,1,0:T(8,128)(2,1)} %query_latent.1, ...), custom_call_target="tpu_custom_call" | custom-call | tf_op jit(solution)/shard_map/layer/pallas_call | solution.py:660
  40.5 0.7 %place.1 = (bf16[32,2048]{1,0:T(8,128)(2,1)}, bf16[4,256]{1,0:T(4,128)(2,1)}, bf16[4,32]{1,0:T(4,128)(2,1)}) custom-call(bf16[32,2048]{1,0:T(8,128)(2,1)S(1)} %get-tuple-element.6.refs_0_, bf16[4,256]{1,0:T(4,128)(2,1)S(1)} %get-tuple-element.7.refs_1_, bf16[4,32]{1,0:T(4,128)(2,1)S(1)} %get-tuple-element.8.refs_2_), custom_call_target="tpu_custom_call" | custom-call | tf_op jit(solution)/shard_map/place/pallas_call | solution.py:602

commit v4 on v3

--- a/solution.py
+++ b/solution.py
@@ -291,17 +291,17 @@
     for s in range(1, seqs):
         ropes[s].wait()
         caches[s].wait()
-        if s == seqs - 1:
-            for kind in expert_loads:
-                for load in kind:
-                    load.start()
+    for kind in expert_loads:
+        for load in kind:
+            load.start()
+    loads[8].wait()
+    for s in range(1, seqs):
         found = scores(s)
         mixed_latents.append(mix(s - 1, *waiting))
         waiting = found
     mixed_latents.append(mix(seqs - 1, *waiting))
     lhs = jnp.concatenate(mixed_latents, axis=0)
 
-    loads[8].wait()
     for t in range(n_tp):
         found = dot(lhs, value_v[:, t * head_cols : (t + 1) * head_cols])
         head = iota((heads, head_cols), 0)

time: 41.3 us -> 40.8 us (0.988)
  Pallas kernels: 40.5 us -> 40 us
    pallas_call x1, Pallas kernels: 39.8 us -> 39.3 us  [on_device(): pl.pallas_call(functools.partial(layer, (n_ep, n_tp, slots, scale)), out_...]
where the time goes in v4:
time: 40.8 us; the launch traced here: 40.6 us
  Pallas kernels  40 us (98%)
  between operations  0.65 us (2%)
    pallas_call x1, Pallas kernels, on_device(): pl.pallas_call(functools.partial(layer, (n_ep, n_tp, slots, scale)), out_...  39.3 us

profile of v4, /device:TPU:0, one launch (start us, length us, event | category | flops | bytes accessed | tf_op | source)
XLA Modules:
  0.0 40.6 jit_solution(3359440249880485853)
XLA Ops:
  0.6 39.3 %layer.1 = (bf16[32,2048]{1,0:T(8,128)(2,1)S(1)}, bf16[4,256]{1,0:T(4,128)(2,1)S(1)}, bf16[4,32]{1,0:T(4,128)(2,1)S(1)}) custom-call(bf16[32,2048]{1,0:T(8,128)(2,1)} %residual.1, bf16[4,2048,256]{2,1,0:T(8,128)(2,1)} %cache_latent.1, bf16[4,32,2048]{2,1,0:T(8,128)(2,1)} %cache_rope.1, s32[4]{0:T(128)} %lengths_hbm.1, bf16[4,32,256]{2,1,0:T(8,128)(2,1)} %query_latent.1, ...), custom_call_target="tpu_custom_call" | custom-call | tf_op jit(solution)/shard_map/layer/pallas_call | solution.py:660
  39.9 0.7 %place.1 = (bf16[32,2048]{1,0:T(8,128)(2,1)}, bf16[4,256]{1,0:T(4,128)(2,1)}, bf16[4,32]{1,0:T(4,128)(2,1)}) custom-call(bf16[32,2048]{1,0:T(8,128)(2,1)S(1)} %get-tuple-element.6.refs_0_, bf16[4,256]{1,0:T(4,128)(2,1)S(1)} %get-tuple-element.7.refs_1_, bf16[4,32]{1,0:T(4,128)(2,1)S(1)} %get-tuple-element.8.refs_2_), custom_call_target="tpu_custom_call" | custom-call | tf_op jit(solution)/shard_map/place/pallas_call | solution.py:602
